TPU v7x, 32 devices: a whole 2x2x4 slice. The times are simulated.
32 devices in a mesh: ep: 32 (over z, y, x, core).
Axes of the slice: x: 2, y: 2, z: 4, core: 2. Of those that a mesh axis runs over, the one named last changes fastest.
Arguments:
- tokens: bfloat16 [640, 2048], P('ep'), may hold values from -6 to 6
- positions: int32 [640], P('ep'), may hold values from 1024 to 16383
- state: float32 [640, 8, 64, 128], P('ep'), may hold values from -1.6 to 1.6
- mix_gain: float32 [2048], replicated, may hold values from 0.1 to 1.9
- w_query: bfloat16 [2048, 512], replicated, may hold values from -0.125 to 0.125
- w_key: bfloat16 [2048, 512], replicated, may hold values from -0.125 to 0.125
- w_value: bfloat16 [2048, 1024], replicated, may hold values from -0.125 to 0.125
- ret_gain: float32 [1024], replicated, may hold values from 0.1 to 1.9
- w_out: bfloat16 [1024, 2048], P(None, 'ep'), may hold values from -0.1875 to 0.1875
- ffn_gain: float32 [2048], replicated, may hold values from 0.1 to 1.9
- routes: int32 [640, 6], P('ep'), may hold values from 0 to 31, all different within a row; in each aligned block of 20 rows (0 to 19, 20 to 39, ...) at most 7 rows name the same one
- route_weights: float32 [640, 6], P('ep'), may hold values from 0.1 to 1
- expert_gate: bfloat16 [32, 2048, 512], P('ep'), may hold values from -0.125 to 0.125
- expert_up: bfloat16 [32, 2048, 512], P('ep'), may hold values from -0.125 to 0.125
- expert_down: bfloat16 [32, 512, 2048], P('ep'), may hold values from -0.25 to 0.25
Outputs:
- result: bfloat16 [640, 2048], P('ep')
- new_state: float32 [640, 8, 64, 128], P('ep')
Inputs may be any that keep to these rules, and one draw needn't show every extreme that they name: `routes`: each row names 6 different experts; among the rows of one device no expert is named more than 7 times, a bound that some block reaches there.
All inputs are finite; a program needn't handle non-finite values.
Results may differ from a plain program's by a relative error of at most 0.017.
Values may be sent and summed in bfloat16 or wider, within the bound.
A program may use at most 128 MiB of HBM per device.

v0:
```python
import functools
import math

import jax
import jax.numpy as jnp
from jax import lax
from jax.experimental import pallas as pl
from jax.experimental.pallas import tpu as pltpu
from jax.sharding import PartitionSpec as P

EPS = 1e-06
MESH = pl.DeviceIdType.MESH
PAD = 8
VMEM_LIMIT = 64 * 1024 * 1024 - 128 * 1024


def layout_of(mesh):
    devices = list(mesh.devices.flat)
    count = len(devices)
    try:
        far = [max(d.coords[i] for d in devices) - min(d.coords[i] for d in devices) + 1 for i in range(3)]
        cores = count // (far[0] * far[1] * far[2])
        if cores * far[0] * far[1] * far[2] == count and cores >= 1:
            return (far[2], far[1], far[0], cores)
    except (AttributeError, TypeError, IndexError):
        pass
    cores = 2 if count % 2 == 0 else 1
    chips = count // cores
    side = 1
    while (side * 2) ** 2 * 4 <= chips and chips % ((side * 2) ** 2) == 0:
        side *= 2
    return (chips // (side * side), side, side, cores)


class Place:
    def __init__(self, dims):
        self.dims = dims
        depth, rows, cols, cores = dims
        me = lax.axis_index("ep")
        self.me = me
        self.spot = (
            me // (rows * cols * cores),
            (me // (cols * cores)) % rows,
            (me // cores) % cols,
            me % cores,
        )

    def at(self, dz, dy, dx, dc=0):
        total = 0
        for size, here, move in zip(self.dims, self.spot, (dz, dy, dx, dc)):
            total = total * size + self.moved(size, here, move)
        return total

    @staticmethod
    def moved(size, here, move):
        if not move % size:
            return here
        if size & (size - 1):
            return (here + move) % size
        bit = 1
        there = here
        while bit < size:
            if abs(move) & bit:
                there = there + bit - 2 * bit * ((here // bit) % 2)
            bit *= 2
        return there

    def greet(self, corners=False):
        depth, rows, cols, cores = self.dims
        moves = [(d, 0, 0, 0) for d in range(1, depth)]
        moves += [(0, d, 0, 0) for d in range(1, rows)]
        moves += [(0, 0, d, 0) for d in range(1, cols)]
        if corners:
            moves += [(0, dy, dx, 0) for dy in range(1, rows) for dx in range(1, cols)]
        moves += [(0, 0, 0, d) for d in range(1, cores)]
        barrier = pltpu.get_barrier_semaphore()
        for move in moves:
            pl.semaphore_signal(barrier, inc=1, device_id=(self.at(*move),), device_id_type=MESH)
        pl.semaphore_wait(barrier, len(moves))


def gather_names(dims):
    depth, rows, cols, cores = dims
    names = []
    for dz in range(depth):
        if dz:
            names.append(("z", dz, 0, 0, 0))
        for dx in range(1, cols):
            names.append(("x", dz, 0, dx, 0))
        for dy in range(1, rows):
            names.append(("y", dz, dy, 0, 0))
            for dx in range(1, cols):
                names.append(("p", dz, dy, dx, 0))
                names.append(("q", dz, dy, dx, 0))
        for dy in range(rows):
            for dx in range(cols):
                for dc in range(1, cores):
                    names.append(("c", dz, dy, dx, dc))
    return {name: i for i, name in enumerate(names)}


class Gather:
    def __init__(self, place, view, send, recv):
        self.place, self.view, self.send, self.recv = place, view, send, recv
        self.names = gather_names(place.dims)
        self.sent = []

    def copy(self, name):
        kind, dz, dy, dx, dc = name
        m = self.names[name]
        back = {"z": (-dz, 0, 0, 0), "x": (0, 0, -dx, 0), "y": (0, -dy, 0, 0)}
        back.update({"p": (0, -dy, 0, 0), "q": (0, 0, -dx, 0), "c": (0, 0, 0, -dc)})
        return m, {"p": 0, "q": 1}.get(kind), self.place.at(*back[kind])

    def put(self, name, held):
        m, half, target = self.copy(name)
        ref = self.view(self.place.at(*held), half)
        c = pltpu.make_async_remote_copy(
            src_ref=ref, dst_ref=ref, send_sem=self.send.at[m], recv_sem=self.recv.at[m],
            device_id=(target,), device_id_type=MESH,
        )
        c.start()
        self.sent.append(c)

    def get(self, name):
        m, half, target = self.copy(name)
        ref = self.view(self.place.at(*name[1:]), half)
        pltpu.make_async_remote_copy(
            src_ref=ref, dst_ref=ref, send_sem=self.send.at[m], recv_sem=self.recv.at[m],
            device_id=(target,), device_id_type=MESH,
        ).wait_recv()

    def mates(self, dz, dy, dx):
        for dc in range(1, self.place.dims[3]):
            self.put(("c", dz, dy, dx, dc), (dz, dy, dx, 0))

    def first(self, dz):
        depth, rows, cols, cores = self.place.dims
        if dz == 0:
            for d in range(1, depth):
                self.put(("z", d, 0, 0, 0), (0, 0, 0, 0))
        else:
            self.get(("z", dz, 0, 0, 0))
        for dx in range(1, cols):
            self.put(("x", dz, 0, dx, 0), (dz, 0, 0, 0))
        for dy in range(1, rows):
            self.put(("y", dz, dy, 0, 0), (dz, 0, 0, 0))
        self.mates(dz, 0, 0)

    def second(self, dz):
        depth, rows, cols, cores = self.place.dims
        for dx in range(1, cols):
            self.get(("x", dz, 0, dx, 0))
            for dy in range(1, rows):
                self.put(("p", dz, dy, dx, 0), (dz, 0, dx, 0))
            self.mates(dz, 0, dx)
        for dy in range(1, rows):
            self.get(("y", dz, dy, 0, 0))
            for dx in range(1, cols):
                self.put(("q", dz, dy, dx, 0), (dz, dy, 0, 0))
            self.mates(dz, dy, 0)

    def third(self, dz):
        depth, rows, cols, cores = self.place.dims
        for dy in range(1, rows):
            for dx in range(1, cols):
                self.get(("p", dz, dy, dx, 0))
                self.get(("q", dz, dy, dx, 0))
                self.mates(dz, dy, dx)

    def fourth(self, dz):
        depth, rows, cols, cores = self.place.dims
        for dy in range(rows):
            for dx in range(cols):
                for dc in range(1, cores):
                    self.get(("c", dz, dy, dx, dc))

    def finish(self):
        for c in self.sent:
            c.wait_send()


def halves(ref, width):
    cut = -(-width // 256) * 128
    spans = {None: (0, width), 0: (0, cut), 1: (cut, width - cut)}

    def view(index, half):
        start, size = spans[half]
        return ref.at[index, :, pl.ds(start, size)]

    return view


def retain_kernel(
    dims, sizes, own, normed, wq_hbm, wk_hbm, wv_hbm, cosine, sine, gain, state_hbm,
    out, key_out, value_out,
    wq, wk, wv, state, flip, qcols, kcols, values, decay, readout, lines, mixed, attended, back,
    load, wload, sload, send, recv,
):
    heads, head_k, head_v = sizes
    place = Place(dims)
    seqs = normed.shape[0]
    depth, rows, cols, cores = dims
    names = retain_names(dims)

    def slot(dz, dc):
        return place.moved(depth, place.spot[0], dz) * cores + place.moved(cores, place.spot[3], dc)

    def remote(name, src, dst, target):
        m = names[name]
        return pltpu.make_async_remote_copy(
            src_ref=src, dst_ref=dst, send_sem=send.at[m], recv_sem=recv.at[m],
            device_id=(place.at(*target),), device_id_type=MESH,
        )

    fill = pltpu.make_async_copy(own, lines.at[slot(0, 0)], load)
    fill.start()
    weights = [
        pltpu.make_async_copy(src, dst, wload.at[i])
        for i, (src, dst) in enumerate([(wq_hbm, wq), (wk_hbm, wk), (wv_hbm, wv)])
    ]
    for copy in weights:
        copy.start()
    taken = pltpu.make_async_copy(state_hbm, state, sload)
    taken.start()
    place.greet(corners=True)
    fill.wait()
    sent = []

    def put(*args):
        copy = remote(*args)
        copy.start()
        sent.append(copy)

    for dz in range(1, depth):
        put(("z", dz), lines.at[slot(0, 0)], lines.at[slot(0, 0)], (-dz, 0, 0, 0))
    for dc in range(1, cores):
        put(("c", 0, dc), lines.at[slot(0, 0)], lines.at[slot(0, 0)], (0, 0, 0, -dc))

    def rotated(field):
        lane = lax.broadcasted_iota(jnp.int32, field.shape, 1) % head_k
        total = field.shape[1]
        ahead = pltpu.roll(field, total - head_k // 2, 1)
        behind = pltpu.roll(field, head_k // 2, 1)
        return field * cosine[...] + jnp.where(lane < head_k // 2, -ahead, behind) * sine[...]

    def columns(field, target):
        flip[...] = jnp.zeros_like(flip)
        flip[pl.ds(0, seqs), :] = field
        target[...] = flip[...].T

    def project(weight):
        part = jnp.dot(normed[...], weight[...], preferred_element_type=jnp.float32)
        return part.astype(jnp.bfloat16).astype(jnp.float32)

    def queries():
        weights[0].wait()
        columns(rotated(project(wq)), qcols)

    def keys():
        weights[1].wait()
        key_out[...] = rotated(project(wk)) * head_k ** (-0.5)
        columns(key_out[...], kcols)

    def others():
        weights[2].wait()
        part = project(wv)
        value_out[...] = part
        for h in range(heads):
            values[:, h, :] = part[:, h * head_v : (h + 1) * head_v]
            decay[pl.ds(h * head_k, head_k), :] = jnp.full((head_k, head_v), 1.0 - 2.0 ** (-2.0 - h), jnp.float32)
        taken.wait()

    def span(start, stop):
        def one(t, carry):
            lane = lax.broadcasted_iota(jnp.int32, qcols.shape, 1)
            query = jnp.sum(jnp.where(lane == t, qcols[...], 0.0), axis=1, keepdims=True)
            key = jnp.sum(jnp.where(lane == t, kcols[...], 0.0), axis=1, keepdims=True)
            value = values[t]
            outer = key.reshape(heads, head_k, 1) * value.reshape(heads, 1, head_v)
            fresh = decay[...] * state[t] + outer.reshape(heads * head_k, head_v)
            readout[t] = jnp.sum((query * fresh).reshape(heads, head_k, head_v), axis=1)
            return carry

        lax.fori_loop(start, stop, one, 0)

    def close():
        for h in range(heads):
            read = readout[:, h, :]
            apart = read - jnp.mean(read, axis=1, keepdims=True)
            variance = jnp.mean(apart * apart, axis=1, keepdims=True)
            lanes = pl.ds(h * head_v, head_v)
            mixed[0, pl.ds(0, seqs), lanes] = (apart * lax.rsqrt(variance + EPS) * gain[:, lanes]).astype(mixed.dtype)

    queries()
    keys()
    others()
    span(0, seqs)
    mixed[0] = jnp.zeros(mixed.shape[1:], mixed.dtype)
    close()
    moves = [(dy, dx) for dy in range(rows) for dx in range(cols)]
    for i, (dy, dx) in enumerate(moves):
        if i:
            put(("m", dy, dx), mixed.at[0], mixed.at[i], (0, -dy, -dx, 0))
    for dz in range(1, depth):
        held = lines.at[slot(dz, 0)]
        remote(("z", dz), held, held, (-dz, 0, 0, 0)).wait_recv()
        for dc in range(1, cores):
            put(("c", dz, dc), held, held, (0, 0, 0, -dc))
    for i, (dy, dx) in enumerate(moves):
        if i:
            remote(("m", dy, dx), mixed.at[0], mixed.at[i], (0, -dy, -dx, 0)).wait_recv()
    for dz in range(depth):
        for dc in range(1, cores):
            held = lines.at[slot(dz, dc)]
            remote(("c", dz, dc), held, held, (0, 0, 0, -dc)).wait_recv()
    tall = mixed.shape[1]
    product = lax.dot_general(
        mixed[...].reshape(len(moves) * tall, mixed.shape[2]),
        lines[...].reshape(-1, lines.shape[2]),
        (((1,), (1,)), ((), ())),
        preferred_element_type=jnp.float32,
    )
    attended[...] = product.astype(attended.dtype).reshape(attended.shape)
    for i, (dy, dx) in enumerate(moves):
        if i:
            put(("r", dy, dx), attended.at[i], back.at[i], (0, dy, dx, 0))
    for i, (dy, dx) in enumerate(moves):
        origin = place.moved(rows, place.spot[1], -dy) * cols + place.moved(cols, place.spot[2], -dx)
        if i:
            remote(("r", dy, dx), attended.at[i], back.at[i], (0, dy, dx, 0)).wait_recv()
        out[origin] = back[i] if i else attended[0]
    for copy in sent:
        copy.wait_send()


def retain_names(dims):
    depth, rows, cols, cores = dims
    names = [("z", dz) for dz in range(1, depth)]
    names += [("c", dz, dc) for dz in range(depth) for dc in range(1, cores)]
    names += [(k, dy, dx) for k in "mr" for dy in range(rows) for dx in range(cols) if dy or dx]
    return {name: i for i, name in enumerate(names)}


def retain(dims, sizes, block, normed, wq, wk, wv, cosine, sine, gain, state, collective):
    heads, head_k, head_v = sizes
    depth, rows, cols, cores = dims
    messages = len(retain_names(dims))
    seqs = normed.shape[0]
    flat = (seqs, heads * head_k, head_v)
    anywhere = pl.BlockSpec(memory_space=pl.ANY)
    here = pl.BlockSpec(memory_space=pltpu.VMEM)
    across = -(-seqs // 128) * 128
    tall = -(-seqs // PAD) * PAD
    some = depth * cores * block.shape[0]
    plane = rows * cols
    return pl.pallas_call(
        functools.partial(retain_kernel, dims, sizes),
        out_shape=(
            jax.ShapeDtypeStruct((plane, tall, some), jnp.bfloat16),
            jax.ShapeDtypeStruct((seqs, heads * head_k), jnp.float32),
            jax.ShapeDtypeStruct((seqs, heads * head_v), jnp.float32),
        ),
        in_specs=[anywhere, here, anywhere, anywhere, anywhere, here, here, here, anywhere],
        out_specs=(here, here, here),
        scratch_shapes=[
            pltpu.VMEM(wq.shape, wq.dtype),
            pltpu.VMEM(wk.shape, wk.dtype),
            pltpu.VMEM(wv.shape, wv.dtype),
            pltpu.VMEM(flat, jnp.float32),
            pltpu.VMEM((across, heads * head_k), jnp.float32),
            pltpu.VMEM((heads * head_k, across), jnp.float32),
            pltpu.VMEM((heads * head_k, across), jnp.float32),
            pltpu.VMEM((seqs, heads, head_v), jnp.float32),
            pltpu.VMEM((heads * head_k, head_v), jnp.float32),
            pltpu.VMEM((seqs, heads, head_v), jnp.float32),
            pltpu.VMEM((depth * cores,) + block.shape, block.dtype),
            pltpu.VMEM((plane, tall, heads * head_v), jnp.bfloat16),
            pltpu.VMEM((plane, tall, some), jnp.bfloat16),
            pltpu.VMEM((plane, tall, some), jnp.bfloat16),
            pltpu.SemaphoreType.DMA,
            pltpu.SemaphoreType.DMA((3,)),
            pltpu.SemaphoreType.DMA,
            pltpu.SemaphoreType.DMA((messages,)),
            pltpu.SemaphoreType.DMA((messages,)),
        ],
        compiler_params=pltpu.CompilerParams(
            collective_id=collective, has_side_effects=True, vmem_limit_bytes=VMEM_LIMIT
        ),
        name="retain",
    )(block, normed, wq, wk, wv, cosine, sine, gain, state.reshape(flat))


class Reduce:
    def __init__(self, place, parts, slots, send, recv):
        self.place, self.parts, self.slots, self.send, self.recv = place, parts, slots, send, recv
        self.names = gather_names(place.dims)
        self.sent = []
        self.width = parts.shape[2]

    def span(self, half):
        cut = self.width // 2
        return {None: pl.ds(0, self.width), 0: pl.ds(0, cut), 1: pl.ds(cut, self.width - cut)}[half]

    def copy(self, name):
        kind, dz, dy, dx, dc = name
        m = self.names[name]
        ahead = {"z": (dz, 0, 0, 0), "x": (0, 0, dx, 0), "y": (0, dy, 0, 0)}
        ahead.update({"p": (0, dy, 0, 0), "q": (0, 0, dx, 0), "c": (0, 0, 0, dc)})
        cols = self.span({"p": 0, "q": 1}.get(kind))
        return pltpu.make_async_remote_copy(
            src_ref=self.parts.at[self.place.at(dz, dy, dx, dc), :, cols],
            dst_ref=self.slots.at[m, :, cols],
            send_sem=self.send.at[m], recv_sem=self.recv.at[m],
            device_id=(self.place.at(*ahead[kind]),), device_id_type=MESH,
        )

    def put(self, name):
        c = self.copy(name)
        c.start()
        self.sent.append(c)

    def get(self, name):
        kind = name[0]
        self.copy(name).wait_recv()
        cols = self.span({"p": 0, "q": 1}.get(kind))
        return self.slots[self.names[name], :, cols].astype(jnp.float32)

    def add(self, index, cols, terms):
        value = self.parts[index, :, cols].astype(jnp.float32)
        for term in terms:
            value = value + term
        self.parts[index, :, cols] = value.astype(self.parts.dtype)

    def zeroth(self, dz):
        depth, rows, cols, cores = self.place.dims
        order = sorted(((dy, dx) for dy in range(rows) for dx in range(cols)), key=lambda o: (not o[0]) + (not o[1]))
        for dy, dx in order:
            for dc in range(1, cores):
                self.put(("c", dz, dy, dx, dc))

    def first(self, dz):
        depth, rows, cols, cores = self.place.dims
        order = sorted(((dy, dx) for dy in range(rows) for dx in range(cols)), key=lambda o: (not o[0]) + (not o[1]))
        for dy, dx in order:
            terms = [self.get(("c", dz, dy, dx, dc)) for dc in range(1, cores)]
            if terms:
                self.add(self.place.at(dz, dy, dx), self.span(None), terms)
            if dy and dx:
                self.put(("p", dz, dy, dx, 0))
                self.put(("q", dz, dy, dx, 0))

    def second(self, dz):
        depth, rows, cols, cores = self.place.dims
        for dx in range(1, cols):
            terms = [self.get(("p", dz, dy, dx, 0)) for dy in range(1, rows)]
            if terms:
                self.add(self.place.at(dz, 0, dx), self.span(0), terms)
            self.put(("x", dz, 0, dx, 0))
        for dy in range(1, rows):
            terms = [self.get(("q", dz, dy, dx, 0)) for dx in range(1, cols)]
            if terms:
                self.add(self.place.at(dz, dy, 0), self.span(1), terms)
            self.put(("y", dz, dy, 0, 0))

    def third(self, dz):
        depth, rows, cols, cores = self.place.dims
        terms = [self.get(("x", dz, 0, dx, 0)) for dx in range(1, cols)]
        terms += [self.get(("y", dz, dy, 0, 0)) for dy in range(1, rows)]
        if dz:
            if terms:
                self.add(self.place.at(dz, 0, 0), self.span(None), terms)
            self.put(("z", dz, 0, 0, 0))
            return None
        value = self.parts[self.place.me].astype(jnp.float32)
        for term in terms:
            value = value + term
        return value

    def finish(self):
        for c in self.sent:
            c.wait_send()


def experts_kernel(
    dims, seqs, width, own, resid, gate_hbm, up_hbm, down_hbm, out,
    held, parts, slots, gate, up, down, mine, load, send, recv, back_send, back_recv,
):
    place = Place(dims)
    depth, rows, cols, cores = dims
    count = math.prod(dims)
    plane = rows * cols * cores
    fills = [
        pltpu.make_async_copy(a, b, load.at[i])
        for i, (a, b) in enumerate(
            [(own, held.at[place.me]), (gate_hbm.at[0], gate), (up_hbm.at[0], up), (down_hbm.at[0], down), (resid, mine)]
        )
    ]
    for fill in fills:
        fill.start()
    place.greet()
    fills[0].wait()
    g = Gather(place, halves(held, held.shape[2]), send, recv)
    r = Reduce(place, parts, slots, back_send, back_recv)
    padded = held.shape[1]
    step = max(1, 192 // padded)
    while plane % step:
        step -= 1

    def serve(dz):
        base = place.moved(depth, place.spot[0], dz) * plane
        extra = held.shape[2] - width
        lane = lax.broadcasted_iota(jnp.int32, (step * padded, extra), 1)
        pick = jnp.logical_or(lane == place.me, lane == place.me + count)
        for k in range(0, plane, step):
            some = held[pl.ds(base + k, step)].reshape(step * padded, held.shape[2])
            rows_in = some[:, :width]
            scale = jnp.sum(
                jnp.where(pick, some[:, width:].astype(jnp.float32), 0.0), axis=1, keepdims=True
            )
            gate_part = jnp.dot(rows_in, gate[...], preferred_element_type=jnp.float32)
            up_part = jnp.dot(rows_in, up[...], preferred_element_type=jnp.float32)
            hidden = (gate_part * jax.nn.sigmoid(gate_part) * up_part).astype(jnp.bfloat16)
            served = jnp.dot(hidden, down[...], preferred_element_type=jnp.float32) * scale
            parts[pl.ds(base + k, step)] = served.astype(jnp.bfloat16).reshape(step, padded, width)

    total = None
    for t in range(depth + 6):
        if t < depth:
            g.first(t)
        if 0 <= t - 1 < depth:
            g.second(t - 1)
        if 0 <= t - 2 < depth:
            g.third(t - 2)
        if 0 <= t - 3 < depth:
            g.fourth(t - 3)
            if t == 3:
                for fill in fills[1:]:
                    fill.wait()
            serve(t - 3)
            r.zeroth(t - 3)
        if 0 <= t - 4 < depth:
            r.first(t - 4)
        if 0 <= t - 5 < depth:
            r.second(t - 5)
        if 0 <= t - 6 < depth:
            value = r.third(t - 6)
            total = value if value is not None else total
    for dz in range(1, depth):
        total = total + r.get(("z", dz, 0, 0, 0))
    out[...] = (mine[...].astype(jnp.float32) + total[:seqs]).astype(out.dtype)
    g.finish()
    r.finish()


def experts(dims, block, resid, gate, up, down, collective):
    count = math.prod(dims)
    seqs, width = resid.shape
    messages = len(gather_names(dims))
    padded = block.shape[0]
    anywhere = pl.BlockSpec(memory_space=pl.ANY)
    return pl.pallas_call(
        functools.partial(experts_kernel, dims, seqs, width),
        out_shape=jax.ShapeDtypeStruct(resid.shape, resid.dtype),
        in_specs=[anywhere] * 5,
        out_specs=pl.BlockSpec(memory_space=pltpu.VMEM),
        scratch_shapes=[
            pltpu.VMEM((count,) + block.shape, block.dtype),
            pltpu.VMEM((count, padded, width), jnp.bfloat16),
            pltpu.VMEM((messages, padded, width), jnp.bfloat16),
            pltpu.VMEM(gate.shape[1:], gate.dtype),
            pltpu.VMEM(up.shape[1:], up.dtype),
            pltpu.VMEM(down.shape[1:], down.dtype),
            pltpu.VMEM(resid.shape, resid.dtype),
            pltpu.SemaphoreType.DMA((5,)),
        ] + [pltpu.SemaphoreType.DMA((messages,))] * 4,
        compiler_params=pltpu.CompilerParams(
            collective_id=collective, has_side_effects=True, vmem_limit_bytes=VMEM_LIMIT
        ),
        name="experts",
    )(block, resid, gate, up, down)


def rms_scale(values, gain):
    wide = values.astype(jnp.float32)
    scaled = wide * lax.rsqrt(jnp.mean(wide * wide, axis=-1, keepdims=True) + EPS)
    return (scaled * gain).astype(jnp.bfloat16)


def padded_rows(rows):
    return jnp.pad(rows, ((0, -(-rows.shape[0] // PAD) * PAD - rows.shape[0]), (0, 0)))


def shards(
    dims,
    tokens,
    positions,
    state,
    mix_gain,
    w_query,
    w_key,
    w_value,
    ret_gain,
    w_out,
    ffn_gain,
    routes,
    route_weights,
    expert_gate,
    expert_up,
    expert_down,
):
    seqs = tokens.shape[0]
    width = tokens.shape[1]
    heads = state.shape[1]
    head_k = state.shape[2]
    head_v = state.shape[3]
    normed_in = rms_scale(tokens, mix_gain)
    half = head_k // 2
    freqs = jnp.exp(-math.log(10000.0) * jnp.arange(half, dtype=jnp.float32) / half)
    angle = positions.astype(jnp.float32)[:, None] * jnp.tile(freqs, 2 * heads)[None, :]
    columns, key_rows, values = retain(
        dims, (heads, head_k, head_v), w_out.T, normed_in, w_query, w_key, w_value,
        jnp.cos(angle), jnp.sin(angle), ret_gain.reshape(1, -1), state, 0,
    )
    key_rows = key_rows.reshape(seqs, heads, head_k)
    values = values.reshape(seqs, heads, head_v)
    decays = 1.0 - jnp.exp2(-2.0 - jnp.arange(heads, dtype=jnp.float32))
    new_state = (
        decays[None, :, None, None] * state + key_rows[:, :, :, None] * values[:, :, None, :]
    )
    count = lax.axis_size("ep")
    columns = columns[:, :seqs].reshape(dims[1] * dims[2], seqs, dims[0], -1)
    attended = jnp.transpose(columns, (1, 2, 0, 3)).reshape(seqs, width)
    resid = (tokens.astype(jnp.float32) + attended.astype(jnp.float32)).astype(jnp.bfloat16)
    normed_mid = rms_scale(resid, ffn_gain)
    ids = jnp.arange(count, dtype=jnp.int32)
    wide_weights = jnp.sum(
        jnp.where(routes[:, :, None] == ids[None, None, :], route_weights[:, :, None], 0.0), axis=1
    )
    high = wide_weights.astype(jnp.bfloat16)
    low = (wide_weights - high.astype(jnp.float32)).astype(jnp.bfloat16)
    fill = -(-2 * count // 128) * 128 - 2 * count
    block = jnp.concatenate(
        [normed_mid, high, low, jnp.zeros((seqs, fill), jnp.bfloat16)], axis=1
    )
    block = padded_rows(block)
    result = experts(dims, block, resid, expert_gate, expert_up, expert_down, 1)
    return (result, new_state)


def solution(mesh):
    placed = (
        P("ep", None),
        P("ep"),
        P("ep", None, None, None),
        P(),
        P(),
        P(),
        P(),
        P(),
        P(None, "ep"),
        P(),
        P("ep", None),
        P("ep", None),
        P("ep", None, None),
        P("ep", None, None),
        P("ep", None, None),
    )
    return jax.shard_map(
        functools.partial(shards, layout_of(mesh)),
        mesh=mesh,
        in_specs=placed,
        out_specs=(P("ep", None), P("ep", None, None, None)),
        check_vma=False,
    )
```

profile of v0, /device:TPU:0, one launch (start us, length us, event | category | flops | bytes accessed | tf_op | source)
XLA Modules:
  0.0 88.8 jit_solution(9876132132345172742)
XLA Ops:
  0.6 0.7 convert_element_type.44
  1.3 1.0 %fusion.3 = f32[20]{0:T(128)S(1)} fusion(bf16[20,2048]{1,0:T(8,128)(2,1)} %param.15), kind=kLoop, calls=%fused_computation.9 | loop fusion | flops 122860 | bytes 82000 | tf_op jit(solution)/shard_map/reduce_sum | solution.py:586
  2.4 0.1 mul.87
  2.4 0.8 select_reduce_fusion
  3.3 0.9 %multiply_sine_fusion = (f32[20,512]{1,0:T(8,128)}, f32[20,512]{1,0:T(8,128)}) fusion(f32[512]{0:T(512)S(1)} %mul.87, f32[20]{0:T(128)S(1)} %convert_element_type.44), kind=kLoop, calls=%fused_computation.16 | loop fusion | flops 10240 | bytes 84048 | tf_op jit(solution)/shard_map/sin | solution.py:623
  4.2 1.6 %fusion.5.normed = bf16[20,2048]{1,0:T(8,128)(2,1)} fusion(bf16[20,2048]{1,0:T(8,128)(2,1)} %param.15, f32[2048]{0:T(1024)} %param.18, f32[20]{0:T(128)S(1)} %add_rsqrt_fusion.1), kind=kLoop, calls=%fused_computation.11 | loop fusion | flops 163840 | bytes 172112 | tf_op jit(solution)/shard_map/convert_element_type | solution.py:587
  5.8 24.6 %retain.1 = (bf16[4,24,512]{2,1,0:T(8,128)(2,1)}, f32[20,512]{1,0:T(8,128)}, f32[20,1024]{1,0:T(8,128)}) custom-call(bf16[64,1024]{1,0:T(8,128)(2,1)} %bitcast.11, bf16[20,2048]{1,0:T(8,128)(2,1)} %fusion.5.normed, bf16[2048,512]{1,0:T(8,128)(2,1)} %wq_hbm.1, bf16[2048,512]{1,0:T(8,128)(2,1)} %wk_hbm.1, bf16[2048,1024]{1,0:T(8,128)(2,1)} %wv_hbm.1, ...), custom_call_target="tpu_custom_call" | custom-call | tf_op jit(solution)/shard_map/retain/pallas_call | solution.py:357
  30.4 1.5 %mul.97 = f32[20,8,64]{2,1,0:T(8,128)} reshape(f32[20,512]{1,0:T(8,128)} %get-tuple-element.6) | data formatting | bytes 81920 | tf_op jit(solution)/shard_map/mul | solution.py:629
  31.9 0.9 %slice_convert_fusion = f32[4,20,512]{2,1,0:T(8,128)S(1)} fusion(bf16[4,24,512]{2,1,0:T(8,128)(2,1)} %get-tuple-element.5), kind=kLoop, calls=%fused_computation.13 | loop fusion | flops 40960 | bytes 245760 | tf_op jit(solution)/shard_map/convert_element_type | solution.py:634
  32.8 0.1 reshape.56
  32.9 0.1 copy.25
  32.9 0.1 reshape.54
  33.0 1.0 %fusion = (f32[20]{0:T(128)S(1)}, bf16[20,2048]{1,0:T(8,128)(2,1)S(1)}) fusion(f32[20,2048]{1,0:T(8,128)S(1)} %reshape.54, bf16[20,2048]{1,0:T(8,128)(2,1)} %param.15), kind=kLoop, calls=%fused_computation.6 | loop fusion | flops 245740 | bytes 327760 | tf_op jit(solution)/shard_map/reduce_sum | solution.py:586
  34.1 0.6 copy-done
  34.7 0.0 copy-done.2
  34.7 0.1 fusion.2
  34.8 0.1 concatenate.3
  34.9 0.7 pad.4.own
  35.5 45.3 %experts.1 = bf16[20,2048]{1,0:T(8,128)(2,1)} custom-call(bf16[24,2176]{1,0:T(8,128)(2,1)} %pad.4.own, bf16[20,2048]{1,0:T(8,128)(2,1)} %copy-done, bf16[1,2048,512]{2,1,0:T(8,128)(2,1)} %gate_hbm.1, bf16[1,2048,512]{2,1,0:T(8,128)(2,1)} %up_hbm.1, bf16[1,512,2048]{2,1,0:T(8,128)(2,1)} %down_hbm.1), custom_call_target="tpu_custom_call" | custom-call | tf_op jit(solution)/shard_map/experts/pallas_call | solution.py:562
  80.8 0.9 %copy.28 = f32[3,8,8,128]{3,2,1,0:T(8,128)S(1)} copy(f32[3,8,8,128]{3,1,2,0:T(8,128)} %bitcast.12) | data formatting | bytes 196608
  81.7 0.0 copy-start.1
  81.8 6.4 %multiply_add_fusion = f32[20,8,64,128]{3,2,1,0:T(8,128)} fusion(f32[20,8,64,128]{3,2,1,0:T(8,128)} %param.17, f32[20,8,128]{2,1,0:T(8,128)S(1)} %slice.4, f32[20,8,64]{2,1,0:T(8,128)} %mul.97, f32[8]{0:T(128)S(1)} %exponential_subtract_fusion), kind=kLoop, calls=%fused_computation | loop fusion | flops 3932160 | bytes 10608672 | tf_op jit(solution)/shard_map/add | solution.py:629
  88.2 0.0 copy-done.1
  88.2 0.6 copy.30
  (10 shorter events, 0.1 us)
Async XLA Ops:
  5.8 28.9 %copy-start.2 = (f32[2048]{0:T(1024)S(1)}, f32[2048]{0:T(1024)}, u32[]{:S(2)}) copy-start(f32[2048]{0:T(1024)} %param.24) | copy-start | bytes 24580
  34.0 0.6 copy-start
  81.7 6.4 %copy-start.1 = (bf16[20,2048]{1,0:T(8,128)(2,1)S(1)}, bf16[20,2048]{1,0:T(8,128)(2,1)}, u32[]{:S(2)}) copy-start(bf16[20,2048]{1,0:T(8,128)(2,1)} %experts.1) | copy-start | bytes 245764
where the time goes:
time: 89.2 us; the launch traced here: 88.8 us
  Pallas kernels  69.8 us (78%)
  other arithmetic  13.5 us (15%)
  local copies, waits for them, and re-layouts  4.73 us (5%)
    pallas_call x1, Pallas kernels, experts(): pl.pallas_call(functools.partial(experts_kernel, dims, seqs, width), out_...  45.3 us
    pallas_call x1, Pallas kernels, retain(): pl.pallas_call(functools.partial(retain_kernel, dims, sizes), out_shape=(...  24.6 us
    add x1, other arithmetic, shards(): decays[None, :, None, None] * state  6.39 us
    unnamed x8, local copies, waits for them, and re-layouts  2.19 us
    reduce_sum x2, other arithmetic, rms_scale(): jnp.mean(wide * wide, axis=-1, keepdims=True) + EPS  2.06 us

commit v1 on v0

v1 whole, which is shorter than its diff:
```python
import functools
import math

import jax
import jax.numpy as jnp
from jax import lax
from jax.experimental import pallas as pl
from jax.experimental.pallas import tpu as pltpu
from jax.sharding import PartitionSpec as P

EPS = 1e-06
MESH = pl.DeviceIdType.MESH
PAD = 8
VMEM_LIMIT = 64 * 1024 * 1024 - 128 * 1024


def layout_of(mesh):
    devices = list(mesh.devices.flat)
    count = len(devices)
    try:
        far = [max(d.coords[i] for d in devices) - min(d.coords[i] for d in devices) + 1 for i in range(3)]
        cores = count // (far[0] * far[1] * far[2])
        if cores * far[0] * far[1] * far[2] == count and cores >= 1:
            return (far[2], far[1], far[0], cores)
    except (AttributeError, TypeError, IndexError):
        pass
    cores = 2 if count % 2 == 0 else 1
    chips = count // cores
    side = 1
    while (side * 2) ** 2 * 4 <= chips and chips % ((side * 2) ** 2) == 0:
        side *= 2
    return (chips // (side * side), side, side, cores)


class Place:
    def __init__(self, dims):
        self.dims = dims
        depth, rows, cols, cores = dims
        me = lax.axis_index("ep")
        self.me = me
        self.spot = (
            me // (rows * cols * cores),
            (me // (cols * cores)) % rows,
            (me // cores) % cols,
            me % cores,
        )

    def at(self, dz, dy, dx, dc=0):
        total = 0
        for size, here, move in zip(self.dims, self.spot, (dz, dy, dx, dc)):
            total = total * size + self.moved(size, here, move)
        return total

    @staticmethod
    def moved(size, here, move):
        if not move % size:
            return here
        if size & (size - 1):
            return (here + move) % size
        bit = 1
        there = here
        while bit < size:
            if abs(move) & bit:
                there = there + bit - 2 * bit * ((here // bit) % 2)
            bit *= 2
        return there

    def greet(self, corners=False):
        depth, rows, cols, cores = self.dims
        moves = [(d, 0, 0, 0) for d in range(1, depth)]
        moves += [(0, d, 0, 0) for d in range(1, rows)]
        moves += [(0, 0, d, 0) for d in range(1, cols)]
        if corners:
            moves += [(0, dy, dx, 0) for dy in range(1, rows) for dx in range(1, cols)]
        moves += [(0, 0, 0, d) for d in range(1, cores)]
        barrier = pltpu.get_barrier_semaphore()
        for move in moves:
            pl.semaphore_signal(barrier, inc=1, device_id=(self.at(*move),), device_id_type=MESH)
        pl.semaphore_wait(barrier, len(moves))


def bits_of(number):
    return [1 << b for b in range(number.bit_length()) if number >> b & 1]


def relay_bit(depth, dz):
    if depth & (depth - 1) or len(bits_of(dz)) < 2:
        return 0
    return bits_of(dz)[0]


def gather_names(dims):
    depth, rows, cols, cores = dims
    names = []
    for dz in range(depth):
        if dz:
            names.append(("z", dz, 0, 0, 0))
        for dx in range(1, cols):
            names.append(("x", dz, 0, dx, 0))
        for dy in range(1, rows):
            names.append(("y", dz, dy, 0, 0))
            for dx in range(1, cols):
                names.append(("p", dz, dy, dx, 0))
                names.append(("q", dz, dy, dx, 0))
        for dy in range(rows):
            for dx in range(cols):
                for dc in range(1, cores):
                    names.append(("c", dz, dy, dx, dc))
    return {name: i for i, name in enumerate(names)}


class Gather:
    def __init__(self, place, view, send, recv, split=True):
        self.place, self.view, self.send, self.recv = place, view, send, recv
        self.names = gather_names(place.dims)
        self.parts = {"p": 0, "q": 1} if split else {"p": None}
        self.sent = []

    def copy(self, name):
        kind, dz, dy, dx, dc = name
        m = self.names[name]
        bit = relay_bit(self.place.dims[0], dz)
        back = {"z": (-(bit or dz), 0, 0, 0), "x": (0, 0, -dx, 0), "y": (0, -dy, 0, 0)}
        back.update({"p": (0, -dy, 0, 0), "q": (0, 0, -dx, 0), "c": (0, 0, 0, -dc)})
        return m, self.parts.get(kind), self.place.at(*back[kind])

    def put(self, name, held):
        m, half, target = self.copy(name)
        ref = self.view(self.place.at(*held), half)
        c = pltpu.make_async_remote_copy(
            src_ref=ref, dst_ref=ref, send_sem=self.send.at[m], recv_sem=self.recv.at[m],
            device_id=(target,), device_id_type=MESH,
        )
        c.start()
        self.sent.append(c)

    def get(self, name):
        m, half, target = self.copy(name)
        ref = self.view(self.place.at(*name[1:]), half)
        pltpu.make_async_remote_copy(
            src_ref=ref, dst_ref=ref, send_sem=self.send.at[m], recv_sem=self.recv.at[m],
            device_id=(target,), device_id_type=MESH,
        ).wait_recv()

    def mates(self, dz, dy, dx):
        for dc in range(1, self.place.dims[3]):
            self.put(("c", dz, dy, dx, dc), (dz, dy, dx, 0))

    def away(self):
        depth = self.place.dims[0]
        for d in range(1, depth):
            if not relay_bit(depth, d):
                self.put(("z", d, 0, 0, 0), (0, 0, 0, 0))

    def arrive(self, dz):
        depth = self.place.dims[0]
        self.get(("z", dz, 0, 0, 0))
        for d in range(1, depth):
            bit = relay_bit(depth, d)
            if bit and d ^ bit == dz:
                self.put(("z", d, 0, 0, 0), (dz, 0, 0, 0))

    def first(self, dz):
        depth, rows, cols, cores = self.place.dims
        if dz:
            self.arrive(dz)
        else:
            self.away()
        for dx in range(1, cols):
            self.put(("x", dz, 0, dx, 0), (dz, 0, 0, 0))
        for dy in range(1, rows):
            self.put(("y", dz, dy, 0, 0), (dz, 0, 0, 0))
        self.mates(dz, 0, 0)

    def second(self, dz):
        depth, rows, cols, cores = self.place.dims
        for dx in range(1, cols):
            self.get(("x", dz, 0, dx, 0))
            for dy in range(1, rows):
                self.put(("p", dz, dy, dx, 0), (dz, 0, dx, 0))
            self.mates(dz, 0, dx)
        for dy in range(1, rows):
            self.get(("y", dz, dy, 0, 0))
            for dx in range(1, cols):
                if "q" in self.parts:
                    self.put(("q", dz, dy, dx, 0), (dz, dy, 0, 0))
            self.mates(dz, dy, 0)

    def third(self, dz):
        depth, rows, cols, cores = self.place.dims
        for dy in range(1, rows):
            for dx in range(1, cols):
                for kind in self.parts:
                    self.get((kind, dz, dy, dx, 0))
                self.mates(dz, dy, dx)

    def fourth(self, dz):
        depth, rows, cols, cores = self.place.dims
        for dy in range(rows):
            for dx in range(cols):
                for dc in range(1, cores):
                    self.get(("c", dz, dy, dx, dc))

    def finish(self):
        for c in self.sent:
            c.wait_send()


def halves(ref, width):
    cut = -(-width // 256) * 128
    spans = {None: (0, width), 0: (0, cut), 1: (cut, width - cut)}

    def view(index, half):
        start, size = spans[half]
        return ref.at[index, :, pl.ds(start, size)]

    return view


def slot_names(dims):
    kept = [name for name in gather_names(dims) if name[0] != "q"]
    table = {name: i for i, name in enumerate(kept)}
    table.update({("q",) + name[1:]: i for name, i in table.items() if name[0] == "p"})
    return table, len(kept)


class Reduce:
    def __init__(self, place, parts, slots, send, recv):
        self.place, self.parts, self.slots, self.send, self.recv = place, parts, slots, send, recv
        self.names = gather_names(place.dims)
        self.places, _ = slot_names(place.dims)
        self.sent = []
        self.width = parts.shape[2]

    def span(self, half):
        cut = self.width // 2
        return {None: pl.ds(0, self.width), 0: pl.ds(0, cut), 1: pl.ds(cut, self.width - cut)}[half]

    def copy(self, name):
        kind, dz, dy, dx, dc = name
        m = self.names[name]
        ahead = {"z": (dz, 0, 0, 0), "x": (0, 0, dx, 0), "y": (0, dy, 0, 0)}
        ahead.update({"p": (0, dy, 0, 0), "q": (0, 0, dx, 0), "c": (0, 0, 0, dc)})
        cols = self.span({"p": 0, "q": 1}.get(kind))
        return pltpu.make_async_remote_copy(
            src_ref=self.parts.at[self.place.at(dz, dy, dx, dc), :, cols],
            dst_ref=self.slots.at[self.places[name], :, cols],
            send_sem=self.send.at[m], recv_sem=self.recv.at[m],
            device_id=(self.place.at(*ahead[kind]),), device_id_type=MESH,
        )

    def put(self, name):
        c = self.copy(name)
        c.start()
        self.sent.append(c)

    def get(self, name):
        kind = name[0]
        self.copy(name).wait_recv()
        cols = self.span({"p": 0, "q": 1}.get(kind))
        return self.slots[self.places[name], :, cols].astype(jnp.float32)

    def add(self, index, cols, terms):
        value = self.parts[index, :, cols].astype(jnp.float32)
        for term in terms:
            value = value + term
        self.parts[index, :, cols] = value.astype(self.parts.dtype)

    def order(self):
        depth, rows, cols, cores = self.place.dims
        return sorted(((dy, dx) for dy in range(rows) for dx in range(cols)), key=lambda o: (not o[0]) + (not o[1]))

    def zeroth(self, dz):
        for dy, dx in self.order():
            for dc in range(1, self.place.dims[3]):
                self.put(("c", dz, dy, dx, dc))

    def first(self, dz):
        for dy, dx in self.order():
            terms = [self.get(("c", dz, dy, dx, dc)) for dc in range(1, self.place.dims[3])]
            if terms:
                self.add(self.place.at(dz, dy, dx), self.span(None), terms)
            if dy and dx:
                self.put(("p", dz, dy, dx, 0))
                self.put(("q", dz, dy, dx, 0))

    def second(self, dz):
        depth, rows, cols, cores = self.place.dims
        for dx in range(1, cols):
            terms = [self.get(("p", dz, dy, dx, 0)) for dy in range(1, rows)]
            if terms:
                self.add(self.place.at(dz, 0, dx), self.span(0), terms)
            self.put(("x", dz, 0, dx, 0))
        for dy in range(1, rows):
            terms = [self.get(("q", dz, dy, dx, 0)) for dx in range(1, cols)]
            if terms:
                self.add(self.place.at(dz, dy, 0), self.span(1), terms)
            self.put(("y", dz, dy, 0, 0))

    def third(self, dz):
        depth, rows, cols, cores = self.place.dims
        terms = [self.get(("x", dz, 0, dx, 0)) for dx in range(1, cols)]
        terms += [self.get(("y", dz, dy, 0, 0)) for dy in range(1, rows)]
        if dz:
            if terms:
                self.add(self.place.at(dz, 0, 0), self.span(None), terms)
            self.put(("z", dz, 0, 0, 0))
            return None
        value = self.parts[self.place.me].astype(jnp.float32)
        for term in terms:
            value = value + term
        return value

    def finish(self):
        for c in self.sent:
            c.wait_send()


def line_names(dims):
    depth, rows, cols, cores = dims
    names = [("z", dz) for dz in range(1, depth)]
    names += [("c", dz, dc) for dz in range(depth) for dc in range(1, cores)]
    names += [(k, dy, dx) for k in "mr" for dy in range(rows) for dx in range(cols) if dy or dx]
    return {name: i for i, name in enumerate(names)}


def rms_scale(wide, gain):
    scaled = wide * lax.rsqrt(jnp.mean(wide * wide, axis=-1, keepdims=True) + EPS)
    return (scaled * gain).astype(jnp.bfloat16)


def layer_kernel(
    dims, sizes, tokens_hbm, spots_hbm, routes_hbm, shares_hbm, gains_hbm, ret_hbm, mids_hbm, own, wq_hbm, wk_hbm, wv_hbm,
    state_hbm, gate_hbm, up_hbm, down_hbm,
    out, state,
    tokens, spots, routes, shares, gains, rets, mids, lanes_i, lanes_f,
    wq, wk, wv, flip, qcols, kcols, values, decay, readout, lines, mixed, attended, back,
    held, scales, parts, slots, gate, up, down, resid, blend, stage, share,
    load, wload, sload, send, recv, gsend, grecv, wsend, wrecv, rsend, rrecv,
):
    heads, head_k, head_v, topk = sizes
    place = Place(dims)
    seqs, width = tokens.shape
    padded = -(-seqs // PAD) * PAD
    depth, rows, cols, cores = dims
    count = math.prod(dims)
    plane = rows * cols * cores
    names = line_names(dims)

    def slot(dz, dc):
        return place.moved(depth, place.spot[0], dz) * cores + place.moved(cores, place.spot[3], dc)

    def remote(name, src, dst, target):
        m = names[name]
        return pltpu.make_async_remote_copy(
            src_ref=src, dst_ref=dst, send_sem=send.at[m], recv_sem=recv.at[m],
            device_id=(place.at(*target),), device_id_type=MESH,
        )

    pairs = [
        (own, lines.at[slot(0, 0)]), (tokens_hbm, tokens), (spots_hbm, spots), (routes_hbm, routes),
        (shares_hbm, shares), (gains_hbm, gains), (ret_hbm, rets), (mids_hbm, mids),
    ]
    fills = [pltpu.make_async_copy(a, b, load.at[i]) for i, (a, b) in enumerate(pairs)]
    for fill in fills:
        fill.start()
    weights = [
        pltpu.make_async_copy(src, dst, wload.at[i])
        for i, (src, dst) in enumerate(
            [(wq_hbm, wq), (wk_hbm, wk), (wv_hbm, wv), (gate_hbm.at[0], gate), (up_hbm.at[0], up), (down_hbm.at[0], down)]
        )
    ]
    for copy in weights[:3]:
        copy.start()
    taken = pltpu.make_async_copy(state_hbm, state, sload)
    taken.start()
    for copy in weights[3:]:
        copy.start()
    place.greet(corners=True)
    sent = []

    def put(*args):
        copy = remote(*args)
        copy.start()
        sent.append(copy)

    def line_target(dz):
        return (-(relay_bit(depth, dz) or dz), 0, 0, 0)

    def line_arrive(dz):
        ref = lines.at[slot(dz, 0)]
        remote(("z", dz), ref, ref, line_target(dz)).wait_recv()
        for d in range(1, depth):
            bit = relay_bit(depth, d)
            if bit and d ^ bit == dz:
                put(("z", d), ref, ref, line_target(d))
        for dc in range(1, cores):
            put(("c", dz, dc), ref, ref, (0, 0, 0, -dc))

    fills[0].wait()
    mine = lines.at[slot(0, 0)]
    for dz in range(1, depth):
        if not relay_bit(depth, dz):
            put(("z", dz), mine, mine, line_target(dz))
    for dc in range(1, cores):
        put(("c", 0, dc), mine, mine, (0, 0, 0, -dc))
    for fill in fills[1:]:
        fill.wait()

    lanes_i[...] = jnp.full(lanes_i.shape, -1, jnp.int32)
    lanes_f[...] = jnp.zeros_like(lanes_f)
    lanes_i[pl.ds(0, topk), pl.ds(0, seqs)] = routes[...]
    lanes_f[pl.ds(0, topk), pl.ds(0, seqs)] = shares[...]
    across = lanes_f.shape[1]
    tall_e = scales.shape[2]
    ids = lax.broadcasted_iota(jnp.int32, (tall_e, across), 0)
    wide_t = jnp.zeros((tall_e, across), jnp.float32)
    for k in range(topk):
        wide_t = wide_t + jnp.where(ids == lanes_i[pl.ds(k, 1), :], lanes_f[pl.ds(k, 1), :], 0.0)
    scales[place.me] = wide_t.T[:seqs]
    w = Gather(place, halves(scales, tall_e), wsend, wrecv, split=False)
    w.first(0)

    lanes_f[pl.ds(0, 1), pl.ds(0, seqs)] = spots[...].astype(jnp.float32)
    spread = jnp.broadcast_to(lanes_f[pl.ds(0, 1), :], (across, across)).T[:padded]
    half = head_k // 2
    index = (lax.broadcasted_iota(jnp.int32, (padded, across), 1) % half).astype(jnp.float32)
    angle = spread * jnp.exp(index * (-math.log(10000.0) / half))
    total = heads * head_k
    cosine = jnp.concatenate([jnp.cos(angle)] * (total // across), axis=1)[:seqs]
    sine = jnp.concatenate([jnp.sin(angle)] * (total // across), axis=1)[:seqs]
    normed = rms_scale(tokens[...].astype(jnp.float32), gains[...])

    def rotated(field):
        lane = lax.broadcasted_iota(jnp.int32, field.shape, 1) % head_k
        ahead = pltpu.roll(field, total - half, 1)
        behind = pltpu.roll(field, half, 1)
        return field * cosine + jnp.where(lane < half, -ahead, behind) * sine

    def columns(field, target):
        flip[...] = jnp.zeros_like(flip)
        flip[pl.ds(0, seqs), :] = field
        target[...] = flip[...].T

    def project(weight):
        part = jnp.dot(normed, weight[...], preferred_element_type=jnp.float32)
        return part.astype(jnp.bfloat16).astype(jnp.float32)

    weights[0].wait()
    columns(rotated(project(wq)), qcols)
    weights[1].wait()
    columns(rotated(project(wk)) * head_k ** (-0.5), kcols)
    weights[2].wait()
    part = project(wv)
    for h in range(heads):
        values[:, h, :] = part[:, h * head_v : (h + 1) * head_v]
        decay[pl.ds(h * head_k, head_k), :] = jnp.full((head_k, head_v), 1.0 - 2.0 ** (-2.0 - h), jnp.float32)
    w.second(0)
    taken.wait()

    def one(t, carry):
        lane = lax.broadcasted_iota(jnp.int32, qcols.shape, 1)
        query = jnp.sum(jnp.where(lane == t, qcols[...], 0.0), axis=1, keepdims=True)
        key = jnp.sum(jnp.where(lane == t, kcols[...], 0.0), axis=1, keepdims=True)
        value = values[t]
        outer = key.reshape(heads, head_k, 1) * value.reshape(heads, 1, head_v)
        fresh = decay[...] * state[t] + outer.reshape(heads * head_k, head_v)
        state[t] = fresh
        readout[t] = jnp.sum((query * fresh).reshape(heads, head_k, head_v), axis=1)
        return carry

    lax.fori_loop(0, seqs, one, 0)
    for h in range(heads):
        read = readout[:, h, :]
        apart = read - jnp.mean(read, axis=1, keepdims=True)
        variance = jnp.mean(apart * apart, axis=1, keepdims=True)
        lanes = pl.ds(h * head_v, head_v)
        mixed[0, :, lanes] = (apart * lax.rsqrt(variance + EPS) * rets[:, lanes]).astype(mixed.dtype)
    moves = [(dy, dx) for dy in range(rows) for dx in range(cols)]
    for i, (dy, dx) in enumerate(moves):
        if i:
            put(("m", dy, dx), mixed.at[0], mixed.at[i], (0, -dy, -dx, 0))
    singles = [dz for dz in range(1, depth) if not relay_bit(depth, dz)]
    relays = [dz for dz in range(1, depth) if relay_bit(depth, dz)]
    for dz in singles:
        line_arrive(dz)
        w.first(dz)
    w.third(0)
    for i, (dy, dx) in enumerate(moves):
        if i:
            remote(("m", dy, dx), mixed.at[0], mixed.at[i], (0, -dy, -dx, 0)).wait_recv()
    for dz in relays:
        line_arrive(dz)
    for dz in range(depth):
        for dc in range(1, cores):
            ref = lines.at[slot(dz, dc)]
            remote(("c", dz, dc), ref, ref, (0, 0, 0, -dc)).wait_recv()
    for i in range(len(moves)):
        blend[pl.ds(i * padded, seqs), :] = mixed[i]
    product = lax.dot_general(
        blend[...],
        lines[...].reshape(-1, lines.shape[2]),
        (((1,), (1,)), ((), ())),
        preferred_element_type=jnp.float32,
    )
    for i in range(len(moves)):
        attended[i] = product[i * padded : i * padded + seqs].astype(attended.dtype)
    for i, (dy, dx) in enumerate(moves):
        if i:
            put(("r", dy, dx), attended.at[i], back.at[i], (0, dy, dx, 0))
    for dz in relays:
        w.first(dz)
    for dz in range(1, depth):
        w.second(dz)
    for i, (dy, dx) in enumerate(moves):
        if i:
            remote(("r", dy, dx), attended.at[i], back.at[i], (0, dy, dx, 0)).wait_recv()
    chunk = cores * own.shape[0]
    y_at, x_at = place.spot[1], place.spot[2]
    arranged = []
    for y in range(rows):
        for x in range(cols):
            piece = jnp.zeros(attended.shape[1:], jnp.float32)
            for i, (dy, dx) in enumerate(moves):
                hit = jnp.logical_and(place.moved(rows, y_at, -dy) == y, place.moved(cols, x_at, -dx) == x)
                source = attended[0] if i == 0 else back[i]
                piece = jnp.where(hit, source.astype(jnp.float32), piece)
            arranged.append(piece)
    joined = jnp.concatenate(
        [a[:, z * chunk : (z + 1) * chunk] for z in range(depth) for a in arranged], axis=1
    )
    kept = (tokens[...].astype(jnp.float32) + joined).astype(jnp.bfloat16)
    resid[...] = kept
    held[place.me] = rms_scale(kept.astype(jnp.float32), mids[...])

    g = Gather(place, halves(held, width), gsend, grecv)
    r = Reduce(place, parts, slots, rsend, rrecv)
    step = stage.shape[0] // padded

    def serve(dz):
        base = place.moved(depth, place.spot[0], dz) * plane
        lane = lax.broadcasted_iota(jnp.int32, (step * padded, tall_e), 1)
        for k in range(0, plane, step):
            for i in range(step):
                stage[pl.ds(i * padded, seqs), :] = held[base + k + i]
                share[pl.ds(i * padded, seqs), :] = scales[base + k + i]
            rows_in = stage[...]
            scale = jnp.sum(jnp.where(lane == place.me, share[...], 0.0), axis=1, keepdims=True)
            gate_part = jnp.dot(rows_in, gate[...], preferred_element_type=jnp.float32)
            up_part = jnp.dot(rows_in, up[...], preferred_element_type=jnp.float32)
            hidden = (gate_part * jax.nn.sigmoid(gate_part) * up_part).astype(jnp.bfloat16)
            served = jnp.dot(hidden, down[...], preferred_element_type=jnp.float32) * scale
            for i in range(step):
                parts[base + k + i] = served[i * padded : i * padded + seqs].astype(jnp.bfloat16)

    result = None
    for t in range(depth + 5):
        if t < depth:
            g.first(t)
        if t == 0:
            for dz in range(1, depth):
                w.third(dz)
            for dz in range(depth):
                w.fourth(dz)
            for copy in weights[3:]:
                copy.wait()
        if 0 <= t - 1 < depth:
            g.second(t - 1)
        if 0 <= t - 2 < depth:
            g.third(t - 2)
        if 0 <= t - 4 < depth:
            r.second(t - 4)
        if 0 <= t - 3 < depth:
            r.first(t - 3)
        if 0 <= t - 2 < depth:
            g.fourth(t - 2)
            serve(t - 2)
            r.zeroth(t - 2)
        if 0 <= t - 5 < depth:
            value = r.third(t - 5)
            result = value if value is not None else result
    for dz in range(1, depth):
        result = result + r.get(("z", dz, 0, 0, 0))
    out[...] = (resid[...].astype(jnp.float32) + result).astype(out.dtype)
    for copy in sent:
        copy.wait_send()
    w.finish()
    g.finish()
    r.finish()


def give_kernel(result, fresh, result_out, fresh_out, sems):
    copies = [
        pltpu.make_async_copy(fresh, fresh_out, sems.at[0]),
        pltpu.make_async_copy(result, result_out, sems.at[1]),
    ]
    for copy in copies:
        copy.start()
    for copy in copies:
        copy.wait()


def shards(
    dims, tokens, positions, state, mix_gain, w_query, w_key, w_value, ret_gain, w_out, ffn_gain,
    routes, route_weights, expert_gate, expert_up, expert_down,
):
    seqs, width = tokens.shape
    heads, head_k, head_v = state.shape[1:]
    topk = routes.shape[1]
    depth, rows, cols, cores = dims
    count = math.prod(dims)
    flat = (seqs, heads * head_k, head_v)
    anywhere = pl.BlockSpec(memory_space=pl.ANY)
    here = pl.BlockSpec(memory_space=pltpu.VMEM)
    across = -(-seqs // 128) * 128
    padded = -(-seqs // PAD) * PAD
    block = w_out.T
    some = depth * cores * block.shape[0]
    plane = rows * cols
    tall_e = -(-count // 128) * 128
    lines = len(line_names(dims))
    messages = len(gather_names(dims))
    step = max(1, 192 // padded)
    while (plane * cores) % step:
        step -= 1
    operands = (
        tokens, positions.reshape(1, -1), routes.T, route_weights.T, mix_gain.reshape(1, -1), ret_gain.reshape(1, -1),
        ffn_gain.reshape(1, -1), block, w_query, w_key, w_value, state.reshape(flat), expert_gate, expert_up, expert_down,
    )
    result, fresh = pl.pallas_call(
        functools.partial(layer_kernel, dims, (heads, head_k, head_v, topk)),
        out_shape=(pltpu.VMEM((seqs, width), jnp.bfloat16), pltpu.VMEM(flat, jnp.float32)),
        in_specs=[anywhere] * len(operands),
        out_specs=(here, here),
        scratch_shapes=[
            pltpu.VMEM((seqs, width), jnp.bfloat16),
            pltpu.VMEM((1, seqs), jnp.int32),
            pltpu.VMEM((topk, seqs), jnp.int32),
            pltpu.VMEM((topk, seqs), jnp.float32),
            pltpu.VMEM((1, width), jnp.float32),
            pltpu.VMEM((1, heads * head_v), jnp.float32),
            pltpu.VMEM((1, width), jnp.float32),
            pltpu.VMEM((8, across), jnp.int32),
            pltpu.VMEM((8, across), jnp.float32),
            pltpu.VMEM(w_query.shape, w_query.dtype),
            pltpu.VMEM(w_key.shape, w_key.dtype),
            pltpu.VMEM(w_value.shape, w_value.dtype),
            pltpu.VMEM((across, heads * head_k), jnp.float32),
            pltpu.VMEM((heads * head_k, across), jnp.float32),
            pltpu.VMEM((heads * head_k, across), jnp.float32),
            pltpu.VMEM((seqs, heads, head_v), jnp.float32),
            pltpu.VMEM((heads * head_k, head_v), jnp.float32),
            pltpu.VMEM((seqs, heads, head_v), jnp.float32),
            pltpu.VMEM((depth * cores,) + block.shape, block.dtype),
            pltpu.VMEM((plane, seqs, heads * head_v), jnp.bfloat16),
            pltpu.VMEM((plane, seqs, some), jnp.bfloat16),
            pltpu.VMEM((plane, seqs, some), jnp.bfloat16),
            pltpu.VMEM((count, seqs, width), jnp.bfloat16),
            pltpu.VMEM((count, seqs, tall_e), jnp.float32),
            pltpu.VMEM((count, seqs, width), jnp.bfloat16),
            pltpu.VMEM((slot_names(dims)[1], seqs, width), jnp.bfloat16),
            pltpu.VMEM(expert_gate.shape[1:], expert_gate.dtype),
            pltpu.VMEM(expert_up.shape[1:], expert_up.dtype),
            pltpu.VMEM(expert_down.shape[1:], expert_down.dtype),
            pltpu.VMEM((seqs, width), jnp.bfloat16),
            pltpu.VMEM((plane * padded, heads * head_v), jnp.bfloat16),
            pltpu.VMEM((step * padded, width), jnp.bfloat16),
            pltpu.VMEM((step * padded, tall_e), jnp.float32),
            pltpu.SemaphoreType.DMA((8,)),
            pltpu.SemaphoreType.DMA((6,)),
            pltpu.SemaphoreType.DMA,
        ] + [pltpu.SemaphoreType.DMA((lines,))] * 2 + [pltpu.SemaphoreType.DMA((messages,))] * 6,
        compiler_params=pltpu.CompilerParams(
            collective_id=0, has_side_effects=True, vmem_limit_bytes=VMEM_LIMIT - 4 * math.prod(flat) - (1 << 19)
        ),
        name="layer",
    )(*operands)
    result, fresh = pl.pallas_call(
        give_kernel,
        out_shape=(
            jax.ShapeDtypeStruct((seqs, width), jnp.bfloat16),
            jax.ShapeDtypeStruct(flat, jnp.float32),
        ),
        in_specs=[here, here],
        out_specs=(anywhere, anywhere),
        scratch_shapes=[pltpu.SemaphoreType.DMA((2,))],
        compiler_params=pltpu.CompilerParams(vmem_limit_bytes=1 << 20),
        name="give",
    )(result, fresh)
    return (result, fresh.reshape(state.shape))


def solution(mesh):
    placed = (
        P("ep", None),
        P("ep"),
        P("ep", None, None, None),
        P(),
        P(),
        P(),
        P(),
        P(),
        P(None, "ep"),
        P(),
        P("ep", None),
        P("ep", None),
        P("ep", None, None),
        P("ep", None, None),
        P("ep", None, None),
    )
    return jax.shard_map(
        functools.partial(shards, layout_of(mesh)),
        mesh=mesh,
        in_specs=placed,
        out_specs=(P("ep", None), P("ep", None, None, None)),
        check_vma=False,
    )
```

time: 89.2 us -> 72.3 us (0.81)
  other arithmetic: 13.5 us -> 0 us
  local copies, waits for them, and re-layouts: 4.73 us -> 0 us
  Pallas kernels: 69.8 us -> 71.5 us
    add x1 -> x0, other arithmetic: 6.39 us -> none  [shards(): decays[None, :, None, None] * state]
    convert_element_type x5 -> x0, other arithmetic: 3.28 us -> none  [the longest x2 1.71 us: rms_scale(): return (scaled * gain).astype(jnp.bfloat16)]
    reduce_sum x3 -> x0, other arithmetic: 2.87 us -> none  [the longest x2 2.06 us: rms_scale(): jnp.mean(wide * wide, axis=-1, keepdims=True) + EPS]
    unnamed x8 -> x0, local copies, waits for them, and re-layouts: 2.19 us -> none
    pallas_call x2, Pallas kernels: 69.8 us -> 71.5 us  [the longest x1 69.1 us: shards(): pl.pallas_call(functools.partial(layer_kernel, dims, (heads, head_k, head...]
    mul x3 -> x0, local copies, waits for them, and re-layouts: 1.6 us -> none  [the longest x2 1.52 us: shards(): key_rows[:, :, :, None] * values[:, :, None, :]]
where the time goes in v1:
time: 72.3 us; the launch traced here: 72.1 us
  Pallas kernels  71.5 us (99%)
    pallas_call x1, Pallas kernels, shards(): pl.pallas_call(functools.partial(layer_kernel, dims, (heads, head_k, head...  69.1 us
    pallas_call x1, Pallas kernels, shards(): pl.pallas_call(give_kernel, out_shape=(jax.ShapeDtypeStruct((seqs, width)...  2.38 us

profile of v1, /device:TPU:0, one launch (start us, length us, event | category | flops | bytes accessed | tf_op | source)
XLA Modules:
  0.0 72.1 jit_solution(7669071990777992177)
XLA Ops:
  0.6 69.1 %layer.1 = (bf16[20,2048]{1,0:T(8,128)(2,1)S(1)}, f32[20,512,128]{2,1,0:T(8,128)S(1)}) custom-call(bf16[20,2048]{1,0:T(8,128)(2,1)} %tokens_hbm.1, s32[1,20]{1,0:T(1,128)} %bitcast.16, s32[6,20]{1,0:T(8,128)} %bitcast.13, f32[6,20]{1,0:T(8,128)} %bitcast.14, f32[1,2048]{1,0:T(1,128)} %bitcast.11, f32[1,1024]{1,0:T(1,128)} %bitcast.15, f32[1,2048]{1,0:T(1,128)} %bitcast.12, ...), custom_call_target="tpu_custom_call" | custom-call | tf_op jit(solution)/shard_map/layer/pallas_call | solution.py:630
  69.8 2.4 %give.1 = (bf16[20,2048]{1,0:T(8,128)(2,1)}, f32[20,512,128]{2,1,0:T(8,128)}) custom-call(bf16[20,2048]{1,0:T(8,128)(2,1)S(1)} %get-tuple-element.6.result, f32[20,512,128]{2,1,0:T(8,128)S(1)} %get-tuple-element.7.fresh), custom_call_target="tpu_custom_call" | custom-call | tf_op jit(solution)/shard_map/give/pallas_call | solution.py:678

commit v2 on v1

--- a/solution.py
+++ b/solution.py
@@ -76,7 +76,11 @@
         barrier = pltpu.get_barrier_semaphore()
         for move in moves:
             pl.semaphore_signal(barrier, inc=1, device_id=(self.at(*move),), device_id_type=MESH)
-        pl.semaphore_wait(barrier, len(moves))
+        return len(moves)
+
+    @staticmethod
+    def met(count):
+        pl.semaphore_wait(pltpu.get_barrier_semaphore(), count)
 
 
 def bits_of(number):
@@ -93,36 +97,43 @@
     depth, rows, cols, cores = dims
     names = []
     for dz in range(depth):
-        if dz:
-            names.append(("z", dz, 0, 0, 0))
-        for dx in range(1, cols):
-            names.append(("x", dz, 0, dx, 0))
-        for dy in range(1, rows):
-            names.append(("y", dz, dy, 0, 0))
+        for half in range(2):
+            if dz:
+                names.append(("z", dz, 0, 0, 0, half))
             for dx in range(1, cols):
-                names.append(("p", dz, dy, dx, 0))
-                names.append(("q", dz, dy, dx, 0))
+                names.append(("x", dz, 0, dx, 0, half))
+            for dy in range(1, rows):
+                names.append(("y", dz, dy, 0, 0, half))
+                for dx in range(1, cols):
+                    names.append(("d", dz, dy, dx, 0, half))
         for dy in range(rows):
             for dx in range(cols):
                 for dc in range(1, cores):
-                    names.append(("c", dz, dy, dx, dc))
+                    names.append(("c", dz, dy, dx, dc, None))
     return {name: i for i, name in enumerate(names)}
 
 
 class Gather:
     def __init__(self, place, view, send, recv, split=True):
         self.place, self.view, self.send, self.recv = place, view, send, recv
+        self.direct = () if split else tuple(range(place.dims[0]))
         self.names = gather_names(place.dims)
-        self.parts = {"p": 0, "q": 1} if split else {"p": None}
+        self.halves = (0, 1) if split else (0,)
+        self.split = split
         self.sent = []
 
     def copy(self, name):
-        kind, dz, dy, dx, dc = name
+        kind, dz, dy, dx, dc, half = name
         m = self.names[name]
-        bit = relay_bit(self.place.dims[0], dz)
-        back = {"z": (-(bit or dz), 0, 0, 0), "x": (0, 0, -dx, 0), "y": (0, -dy, 0, 0)}
-        back.update({"p": (0, -dy, 0, 0), "q": (0, 0, -dx, 0), "c": (0, 0, 0, -dc)})
-        return m, self.parts.get(kind), self.place.at(*back[kind])
+        bit = self.relay(dz)
+        back = {"z": (-(bit or dz), 0, 0, 0), "x": (0, 0, -dx, 0), "y": (0, -dy, 0, 0), "c": (0, 0, 0, -dc)}
+        back["d"] = (0, 0, -dx, 0) if half else (0, -dy, 0, 0)
+        if dz in self.direct:
+            back["d"] = (0, -dy, -dx, 0)
+        return m, half if self.split else None, self.place.at(*back[kind])
+
+    def relay(self, dz):
+        return relay_bit(self.place.dims[0], dz) if self.split else 0
 
     def put(self, name, held):
         m, half, target = self.copy(name)
@@ -136,7 +147,7 @@
 
     def get(self, name):
         m, half, target = self.copy(name)
-        ref = self.view(self.place.at(*name[1:]), half)
+        ref = self.view(self.place.at(*name[1:5]), half)
         pltpu.make_async_remote_copy(
             src_ref=ref, dst_ref=ref, send_sem=self.send.at[m], recv_sem=self.recv.at[m],
             device_id=(target,), device_id_type=MESH,
@@ -144,54 +155,62 @@
 
     def mates(self, dz, dy, dx):
         for dc in range(1, self.place.dims[3]):
-            self.put(("c", dz, dy, dx, dc), (dz, dy, dx, 0))
+            self.put(("c", dz, dy, dx, dc, None), (dz, dy, dx, 0))
 
     def away(self):
         depth = self.place.dims[0]
-        for d in range(1, depth):
-            if not relay_bit(depth, d):
-                self.put(("z", d, 0, 0, 0), (0, 0, 0, 0))
-
-    def arrive(self, dz):
+        for d in reversed(range(1, depth)):
+            if not self.relay(d):
+                for half in self.halves:
+                    self.put(("z", d, 0, 0, 0, half), (0, 0, 0, 0))
+
+    def spread(self, dz, half):
+        depth, rows, cols, cores = self.place.dims
+        for dx in range(1, cols):
+            self.put(("x", dz, 0, dx, 0, half), (dz, 0, 0, 0))
+        for dy in range(1, rows):
+            self.put(("y", dz, dy, 0, 0, half), (dz, 0, 0, 0))
+        if dz in self.direct:
+            for dy in range(1, rows):
+                for dx in range(1, cols):
+                    self.put(("d", dz, dy, dx, 0, half), (dz, 0, 0, 0))
+
+    def first(self, dz):
         depth = self.place.dims[0]
-        self.get(("z", dz, 0, 0, 0))
-        for d in range(1, depth):
-            bit = relay_bit(depth, d)
-            if bit and d ^ bit == dz:
-                self.put(("z", d, 0, 0, 0), (dz, 0, 0, 0))
-
-    def first(self, dz):
-        depth, rows, cols, cores = self.place.dims
-        if dz:
-            self.arrive(dz)
-        else:
-            self.away()
-        for dx in range(1, cols):
-            self.put(("x", dz, 0, dx, 0), (dz, 0, 0, 0))
-        for dy in range(1, rows):
-            self.put(("y", dz, dy, 0, 0), (dz, 0, 0, 0))
+        for half in self.halves:
+            if dz:
+                self.get(("z", dz, 0, 0, 0, half))
+                for d in range(1, depth):
+                    bit = self.relay(d)
+                    if bit and d ^ bit == dz:
+                        self.put(("z", d, 0, 0, 0, half), (dz, 0, 0, 0))
+            self.spread(dz, half)
         self.mates(dz, 0, 0)
 
     def second(self, dz):
         depth, rows, cols, cores = self.place.dims
-        for dx in range(1, cols):
-            self.get(("x", dz, 0, dx, 0))
+        for half in self.halves:
+            for dx in range(1, cols):
+                self.get(("x", dz, 0, dx, 0, half))
+                if half == 0 and dz not in self.direct:
+                    for dy in range(1, rows):
+                        self.put(("d", dz, dy, dx, 0, 0), (dz, 0, dx, 0))
+                if half == self.halves[-1]:
+                    self.mates(dz, 0, dx)
             for dy in range(1, rows):
-                self.put(("p", dz, dy, dx, 0), (dz, 0, dx, 0))
-            self.mates(dz, 0, dx)
-        for dy in range(1, rows):
-            self.get(("y", dz, dy, 0, 0))
-            for dx in range(1, cols):
-                if "q" in self.parts:
-                    self.put(("q", dz, dy, dx, 0), (dz, dy, 0, 0))
-            self.mates(dz, dy, 0)
+                self.get(("y", dz, dy, 0, 0, half))
+                if half == 1 and dz not in self.direct:
+                    for dx in range(1, cols):
+                        self.put(("d", dz, dy, dx, 0, 1), (dz, dy, 0, 0))
+                if half == self.halves[-1]:
+                    self.mates(dz, dy, 0)
 
     def third(self, dz):
         depth, rows, cols, cores = self.place.dims
         for dy in range(1, rows):
             for dx in range(1, cols):
-                for kind in self.parts:
-                    self.get((kind, dz, dy, dx, 0))
+                for half in self.halves:
+                    self.get(("d", dz, dy, dx, 0, half))
                 self.mates(dz, dy, dx)
 
     def fourth(self, dz):
@@ -199,7 +218,7 @@
         for dy in range(rows):
             for dx in range(cols):
                 for dc in range(1, cores):
-                    self.get(("c", dz, dy, dx, dc))
+                    self.get(("c", dz, dy, dx, dc, None))
 
     def finish(self):
         for c in self.sent:
@@ -218,17 +237,17 @@
 
 
 def slot_names(dims):
-    kept = [name for name in gather_names(dims) if name[0] != "q"]
-    table = {name: i for i, name in enumerate(kept)}
-    table.update({("q",) + name[1:]: i for name, i in table.items() if name[0] == "p"})
-    return table, len(kept)
+    table = {}
+    for name in gather_names(dims):
+        table.setdefault(name[:5], len(table))
+    return table
 
 
 class Reduce:
     def __init__(self, place, parts, slots, send, recv):
         self.place, self.parts, self.slots, self.send, self.recv = place, parts, slots, send, recv
         self.names = gather_names(place.dims)
-        self.places, _ = slot_names(place.dims)
+        self.places = slot_names(place.dims)
         self.sent = []
         self.width = parts.shape[2]
 
@@ -237,14 +256,14 @@
         return {None: pl.ds(0, self.width), 0: pl.ds(0, cut), 1: pl.ds(cut, self.width - cut)}[half]
 
     def copy(self, name):
-        kind, dz, dy, dx, dc = name
+        kind, dz, dy, dx, dc, half = name
         m = self.names[name]
-        ahead = {"z": (dz, 0, 0, 0), "x": (0, 0, dx, 0), "y": (0, dy, 0, 0)}
-        ahead.update({"p": (0, dy, 0, 0), "q": (0, 0, dx, 0), "c": (0, 0, 0, dc)})
-        cols = self.span({"p": 0, "q": 1}.get(kind))
+        ahead = {"z": (dz, 0, 0, 0), "x": (0, 0, dx, 0), "y": (0, dy, 0, 0), "c": (0, 0, 0, dc)}
+        ahead["d"] = (0, 0, dx, 0) if half else (0, dy, 0, 0)
+        cols = self.span(half)
         return pltpu.make_async_remote_copy(
             src_ref=self.parts.at[self.place.at(dz, dy, dx, dc), :, cols],
-            dst_ref=self.slots.at[self.places[name], :, cols],
+            dst_ref=self.slots.at[self.places[name[:5]], :, cols],
             send_sem=self.send.at[m], recv_sem=self.recv.at[m],
             device_id=(self.place.at(*ahead[kind]),), device_id_type=MESH,
         )
@@ -255,10 +274,8 @@
         self.sent.append(c)
 
     def get(self, name):
-        kind = name[0]
         self.copy(name).wait_recv()
-        cols = self.span({"p": 0, "q": 1}.get(kind))
-        return self.slots[self.places[name], :, cols].astype(jnp.float32)
+        return self.slots[self.places[name[:5]], :, self.span(name[5])].astype(jnp.float32)
 
     def add(self, index, cols, terms):
         value = self.parts[index, :, cols].astype(jnp.float32)
@@ -273,42 +290,48 @@
     def zeroth(self, dz):
         for dy, dx in self.order():
             for dc in range(1, self.place.dims[3]):
-                self.put(("c", dz, dy, dx, dc))
+                self.put(("c", dz, dy, dx, dc, None))
 
     def first(self, dz):
         for dy, dx in self.order():
-            terms = [self.get(("c", dz, dy, dx, dc)) for dc in range(1, self.place.dims[3])]
+            terms = [self.get(("c", dz, dy, dx, dc, None)) for dc in range(1, self.place.dims[3])]
             if terms:
                 self.add(self.place.at(dz, dy, dx), self.span(None), terms)
             if dy and dx:
-                self.put(("p", dz, dy, dx, 0))
-                self.put(("q", dz, dy, dx, 0))
+                self.put(("d", dz, dy, dx, 0, 0))
+                self.put(("d", dz, dy, dx, 0, 1))
+            elif dx:
+                self.put(("x", dz, 0, dx, 0, 1))
+            elif dy:
+                self.put(("y", dz, dy, 0, 0, 0))
 
     def second(self, dz):
         depth, rows, cols, cores = self.place.dims
         for dx in range(1, cols):
-            terms = [self.get(("p", dz, dy, dx, 0)) for dy in range(1, rows)]
+            terms = [self.get(("d", dz, dy, dx, 0, 0)) for dy in range(1, rows)]
             if terms:
                 self.add(self.place.at(dz, 0, dx), self.span(0), terms)
-            self.put(("x", dz, 0, dx, 0))
+            self.put(("x", dz, 0, dx, 0, 0))
         for dy in range(1, rows):
-            terms = [self.get(("q", dz, dy, dx, 0)) for dx in range(1, cols)]
+            terms = [self.get(("d", dz, dy, dx, 0, 1)) for dx in range(1, cols)]
             if terms:
                 self.add(self.place.at(dz, dy, 0), self.span(1), terms)
-            self.put(("y", dz, dy, 0, 0))
+            self.put(("y", dz, dy, 0, 0, 1))
 
     def third(self, dz):
         depth, rows, cols, cores = self.place.dims
-        terms = [self.get(("x", dz, 0, dx, 0)) for dx in range(1, cols)]
-        terms += [self.get(("y", dz, dy, 0, 0)) for dy in range(1, rows)]
-        if dz:
+        for half in range(2):
+            terms = [self.get(("x", dz, 0, dx, 0, half)) for dx in range(1, cols)]
+            terms += [self.get(("y", dz, dy, 0, 0, half)) for dy in range(1, rows)]
             if terms:
-                self.add(self.place.at(dz, 0, 0), self.span(None), terms)
-            self.put(("z", dz, 0, 0, 0))
-            return None
-        value = self.parts[self.place.me].astype(jnp.float32)
-        for term in terms:
-            value = value + term
+                self.add(self.place.at(dz, 0, 0), self.span(half), terms)
+            if dz:
+                self.put(("z", dz, 0, 0, 0, half))
+
+    def total(self, half):
+        value = self.parts[self.place.me, :, self.span(half)].astype(jnp.float32)
+        for dz in range(1, self.place.dims[0]):
+            value = value + self.get(("z", dz, 0, 0, 0, half))
         return value
 
     def finish(self):
@@ -316,11 +339,50 @@
             c.wait_send()
 
 
+def plan(depth):
+    relays = [dz for dz in range(1, depth) if relay_bit(depth, dz)]
+    order = [0] + [dz for dz in reversed(range(1, depth)) if dz not in relays] + relays
+    steps = []
+
+    def say(kind, *planes):
+        for dz in planes:
+            if (kind, dz) not in steps:
+                steps.append((kind, dz))
+
+    say("away", 0)
+    say("first", 0)
+    say("second", 0)
+    say("first", *[dz for dz in order[1:] if dz not in relays])
+    for i, dz in enumerate(order):
+        if i >= 1:
+            say("second", dz)
+            say("first", *relays)
+            say("second", *order[i + 1 : i + 2])
+        say("third", dz)
+        if i >= 2:
+            say("add1", order[i - 1])
+        if i >= 3:
+            say("add2", order[i - 2])
+        say("fourth", dz)
+        say("serve", dz)
+    say("add1", *order[1:])
+    say("add2", *order[-2:-1])
+    say("add3", *order[1:-2])
+    say("add1", 0)
+    say("add2", *order[1:])
+    say("add3", *order[1:-1])
+    say("add2", 0)
+    say("add3", *order[1:], 0)
+    return steps
+
+
 def line_names(dims):
     depth, rows, cols, cores = dims
-    names = [("z", dz) for dz in range(1, depth)]
+    names = [("z", dz, half) for dz in range(1, depth) for half in range(2)]
     names += [("c", dz, dc) for dz in range(depth) for dc in range(1, cores)]
-    names += [(k, dy, dx) for k in "mr" for dy in range(rows) for dx in range(cols) if dy or dx]
+    moves = [(dy, dx) for dy in range(rows) for dx in range(cols) if dy or dx]
+    names += [("m", dy, dx) for dy, dx in moves]
+    names += [("r", dz, dy, dx) for dz in range(depth) for dy, dx in moves]
     return {name: i for i, name in enumerate(names)}
 
 
@@ -370,13 +432,13 @@
             [(wq_hbm, wq), (wk_hbm, wk), (wv_hbm, wv), (gate_hbm.at[0], gate), (up_hbm.at[0], up), (down_hbm.at[0], down)]
         )
     ]
-    for copy in weights[:3]:
+    for copy in weights[:2]:
         copy.start()
+    partners = place.greet(corners=True)
+    for fill in fills:
+        fill.wait()
     taken = pltpu.make_async_copy(state_hbm, state, sload)
-    taken.start()
-    for copy in weights[3:]:
-        copy.start()
-    place.greet(corners=True)
+    weights[2].start()
     sent = []
 
     def put(*args):
@@ -387,25 +449,26 @@
     def line_target(dz):
         return (-(relay_bit(depth, dz) or dz), 0, 0, 0)
 
-    def line_arrive(dz):
-        ref = lines.at[slot(dz, 0)]
-        remote(("z", dz), ref, ref, line_target(dz)).wait_recv()
+    def line_part(dz, half):
+        rows_there = lines.shape[1] // 2
+        return lines.at[slot(dz, 0), pl.ds(half * rows_there, rows_there)]
+
+    def line_send(dz, half, held):
+        ref = line_part(held, half)
+        put(("z", dz, half), ref, ref, line_target(dz))
+
+    def line_arrive(dz, half):
+        ref = line_part(dz, half)
+        remote(("z", dz, half), ref, ref, line_target(dz)).wait_recv()
         for d in range(1, depth):
             bit = relay_bit(depth, d)
             if bit and d ^ bit == dz:
-                put(("z", d), ref, ref, line_target(d))
+                line_send(d, half, dz)
+
+    def line_mates(dz):
+        ref = lines.at[slot(dz, 0)]
         for dc in range(1, cores):
             put(("c", dz, dc), ref, ref, (0, 0, 0, -dc))
-
-    fills[0].wait()
-    mine = lines.at[slot(0, 0)]
-    for dz in range(1, depth):
-        if not relay_bit(depth, dz):
-            put(("z", dz), mine, mine, line_target(dz))
-    for dc in range(1, cores):
-        put(("c", 0, dc), mine, mine, (0, 0, 0, -dc))
-    for fill in fills[1:]:
-        fill.wait()
 
     lanes_i[...] = jnp.full(lanes_i.shape, -1, jnp.int32)
     lanes_f[...] = jnp.zeros_like(lanes_f)
@@ -418,24 +481,30 @@
     for k in range(topk):
         wide_t = wide_t + jnp.where(ids == lanes_i[pl.ds(k, 1), :], lanes_f[pl.ds(k, 1), :], 0.0)
     scales[place.me] = wide_t.T[:seqs]
-    w = Gather(place, halves(scales, tall_e), wsend, wrecv, split=False)
-    w.first(0)
-
     lanes_f[pl.ds(0, 1), pl.ds(0, seqs)] = spots[...].astype(jnp.float32)
     spread = jnp.broadcast_to(lanes_f[pl.ds(0, 1), :], (across, across)).T[:padded]
-    half = head_k // 2
-    index = (lax.broadcasted_iota(jnp.int32, (padded, across), 1) % half).astype(jnp.float32)
-    angle = spread * jnp.exp(index * (-math.log(10000.0) / half))
+    turn = head_k // 2
+    index = (lax.broadcasted_iota(jnp.int32, (padded, across), 1) % turn).astype(jnp.float32)
+    angle = spread * jnp.exp(index * (-math.log(10000.0) / turn))
     total = heads * head_k
     cosine = jnp.concatenate([jnp.cos(angle)] * (total // across), axis=1)[:seqs]
     sine = jnp.concatenate([jnp.sin(angle)] * (total // across), axis=1)[:seqs]
     normed = rms_scale(tokens[...].astype(jnp.float32), gains[...])
+    Place.met(partners)
+    w = Gather(place, halves(scales, tall_e), wsend, wrecv, split=False)
+    w.away()
+    w.first(0)
+    for dz in reversed(range(1, depth)):
+        if not relay_bit(depth, dz):
+            for half in range(2):
+                line_send(dz, half, 0)
+    line_mates(0)
 
     def rotated(field):
         lane = lax.broadcasted_iota(jnp.int32, field.shape, 1) % head_k
-        ahead = pltpu.roll(field, total - half, 1)
-        behind = pltpu.roll(field, half, 1)
-        return field * cosine + jnp.where(lane < half, -ahead, behind) * sine
+        ahead = pltpu.roll(field, total - turn, 1)
+        behind = pltpu.roll(field, turn, 1)
+        return field * cosine + jnp.where(lane < turn, -ahead, behind) * sine
 
     def columns(field, target):
         flip[...] = jnp.zeros_like(flip)
@@ -446,8 +515,11 @@
         part = jnp.dot(normed, weight[...], preferred_element_type=jnp.float32)
         return part.astype(jnp.bfloat16).astype(jnp.float32)
 
+    singles = [dz for dz in reversed(range(1, depth)) if not relay_bit(depth, dz)]
+    relays = [dz for dz in range(1, depth) if relay_bit(depth, dz)]
     weights[0].wait()
     columns(rotated(project(wq)), qcols)
+    taken.start()
     weights[1].wait()
     columns(rotated(project(wk)) * head_k ** (-0.5), kcols)
     weights[2].wait()
@@ -455,7 +527,6 @@
     for h in range(heads):
         values[:, h, :] = part[:, h * head_v : (h + 1) * head_v]
         decay[pl.ds(h * head_k, head_k), :] = jnp.full((head_k, head_v), 1.0 - 2.0 ** (-2.0 - h), jnp.float32)
-    w.second(0)
     taken.wait()
 
     def one(t, carry):
@@ -469,7 +540,14 @@
         readout[t] = jnp.sum((query * fresh).reshape(heads, head_k, head_v), axis=1)
         return carry
 
-    lax.fori_loop(0, seqs, one, 0)
+    lax.fori_loop(0, seqs // 2, one, 0, unroll=2)
+    for dz in singles[:1]:
+        line_arrive(dz, 0)
+    for dz in range(1, depth):
+        w.first(dz)
+    for copy in weights[3:]:
+        copy.start()
+    lax.fori_loop(seqs // 2, seqs, one, 0, unroll=2)
     for h in range(heads):
         read = readout[:, h, :]
         apart = read - jnp.mean(read, axis=1, keepdims=True)
@@ -480,55 +558,58 @@
     for i, (dy, dx) in enumerate(moves):
         if i:
             put(("m", dy, dx), mixed.at[0], mixed.at[i], (0, -dy, -dx, 0))
-    singles = [dz for dz in range(1, depth) if not relay_bit(depth, dz)]
-    relays = [dz for dz in range(1, depth) if relay_bit(depth, dz)]
-    for dz in singles:
-        line_arrive(dz)
-        w.first(dz)
-    w.third(0)
+    for i, dz in enumerate(singles):
+        for half in range(0 if i else 1, 2):
+            line_arrive(dz, half)
+        line_mates(dz)
+    for dz in range(depth):
+        w.second(dz)
+        w.third(dz)
     for i, (dy, dx) in enumerate(moves):
         if i:
             remote(("m", dy, dx), mixed.at[0], mixed.at[i], (0, -dy, -dx, 0)).wait_recv()
-    for dz in relays:
-        line_arrive(dz)
-    for dz in range(depth):
+    for i in range(len(moves)):
+        blend[pl.ds(i * padded, seqs), :] = mixed[i]
+
+    def attend(dz):
+        at = place.moved(depth, place.spot[0], dz)
         for dc in range(1, cores):
             ref = lines.at[slot(dz, dc)]
             remote(("c", dz, dc), ref, ref, (0, 0, 0, -dc)).wait_recv()
-    for i in range(len(moves)):
-        blend[pl.ds(i * padded, seqs), :] = mixed[i]
-    product = lax.dot_general(
-        blend[...],
-        lines[...].reshape(-1, lines.shape[2]),
-        (((1,), (1,)), ((), ())),
-        preferred_element_type=jnp.float32,
-    )
-    for i in range(len(moves)):
-        attended[i] = product[i * padded : i * padded + seqs].astype(attended.dtype)
-    for i, (dy, dx) in enumerate(moves):
-        if i:
-            put(("r", dy, dx), attended.at[i], back.at[i], (0, dy, dx, 0))
+        product = lax.dot_general(
+            blend[...],
+            lines[pl.ds(at * cores, cores)].reshape(-1, lines.shape[2]),
+            (((1,), (1,)), ((), ())),
+            preferred_element_type=jnp.float32,
+        )
+        for i, (dy, dx) in enumerate(moves):
+            attended[at, i] = product[i * padded : i * padded + seqs].astype(attended.dtype)
+            if i:
+                put(("r", dz, dy, dx), attended.at[at, i], back.at[at, i], (0, dy, dx, 0))
+
     for dz in relays:
-        w.first(dz)
-    for dz in range(1, depth):
-        w.second(dz)
-    for i, (dy, dx) in enumerate(moves):
-        if i:
-            remote(("r", dy, dx), attended.at[i], back.at[i], (0, dy, dx, 0)).wait_recv()
-    chunk = cores * own.shape[0]
+        for half in range(2):
+            line_arrive(dz, half)
+        line_mates(dz)
+    for dz in [0] + singles + relays:
+        attend(dz)
+    for dz in [0] + singles + relays:
+        at = place.moved(depth, place.spot[0], dz)
+        for i, (dy, dx) in enumerate(moves):
+            if i:
+                remote(("r", dz, dy, dx), attended.at[at, i], back.at[at, i], (0, dy, dx, 0)).wait_recv()
     y_at, x_at = place.spot[1], place.spot[2]
-    arranged = []
-    for y in range(rows):
-        for x in range(cols):
-            piece = jnp.zeros(attended.shape[1:], jnp.float32)
-            for i, (dy, dx) in enumerate(moves):
-                hit = jnp.logical_and(place.moved(rows, y_at, -dy) == y, place.moved(cols, x_at, -dx) == x)
-                source = attended[0] if i == 0 else back[i]
-                piece = jnp.where(hit, source.astype(jnp.float32), piece)
-            arranged.append(piece)
-    joined = jnp.concatenate(
-        [a[:, z * chunk : (z + 1) * chunk] for z in range(depth) for a in arranged], axis=1
-    )
+    pieces = []
+    for z in range(depth):
+        found = [(attended if i == 0 else back)[z, i].astype(jnp.float32) for i in range(len(moves))]
+        for y in range(rows):
+            for x in range(cols):
+                piece = found[0]
+                for i, (dy, dx) in enumerate(moves):
+                    hit = jnp.logical_and(place.moved(rows, y_at, -dy) == y, place.moved(cols, x_at, -dx) == x)
+                    piece = jnp.where(hit, found[i], piece)
+                pieces.append(piece)
+    joined = jnp.concatenate(pieces, axis=1)
     kept = (tokens[...].astype(jnp.float32) + joined).astype(jnp.bfloat16)
     resid[...] = kept
     held[place.me] = rms_scale(kept.astype(jnp.float32), mids[...])
@@ -553,35 +634,24 @@
             for i in range(step):
                 parts[base + k + i] = served[i * padded : i * padded + seqs].astype(jnp.bfloat16)
 
-    result = None
-    for t in range(depth + 5):
-        if t < depth:
-            g.first(t)
-        if t == 0:
-            for dz in range(1, depth):
-                w.third(dz)
-            for dz in range(depth):
-                w.fourth(dz)
-            for copy in weights[3:]:
-                copy.wait()
-        if 0 <= t - 1 < depth:
-            g.second(t - 1)
-        if 0 <= t - 2 < depth:
-            g.third(t - 2)
-        if 0 <= t - 4 < depth:
-            r.second(t - 4)
-        if 0 <= t - 3 < depth:
-            r.first(t - 3)
-        if 0 <= t - 2 < depth:
-            g.fourth(t - 2)
-            serve(t - 2)
-            r.zeroth(t - 2)
-        if 0 <= t - 5 < depth:
-            value = r.third(t - 5)
-            result = value if value is not None else result
-    for dz in range(1, depth):
-        result = result + r.get(("z", dz, 0, 0, 0))
-    out[...] = (resid[...].astype(jnp.float32) + result).astype(out.dtype)
+    for kind, dz in plan(depth):
+        if kind == "serve":
+            if dz == 0:
+                for other in range(depth):
+                    w.fourth(other)
+                for copy in weights[3:]:
+                    copy.wait()
+            serve(dz)
+            r.zeroth(dz)
+        else:
+            act = {
+                "away": lambda _: g.away(), "first": g.first, "second": g.second, "third": g.third,
+                "fourth": g.fourth, "add1": r.first, "add2": r.second, "add3": r.third,
+            }
+            act[kind](dz)
+    for half in range(2):
+        cols_at = r.span(half)
+        out[:, cols_at] = (resid[:, cols_at].astype(jnp.float32) + r.total(half)).astype(out.dtype)
     for copy in sent:
         copy.wait_send()
     w.finish()
@@ -653,12 +723,12 @@
             pltpu.VMEM((seqs, heads, head_v), jnp.float32),
             pltpu.VMEM((depth * cores,) + block.shape, block.dtype),
             pltpu.VMEM((plane, seqs, heads * head_v), jnp.bfloat16),
-            pltpu.VMEM((plane, seqs, some), jnp.bfloat16),
-            pltpu.VMEM((plane, seqs, some), jnp.bfloat16),
+            pltpu.VMEM((depth, plane, seqs, some // depth), jnp.bfloat16),
+            pltpu.VMEM((depth, plane, seqs, some // depth), jnp.bfloat16),
             pltpu.VMEM((count, seqs, width), jnp.bfloat16),
             pltpu.VMEM((count, seqs, tall_e), jnp.float32),
             pltpu.VMEM((count, seqs, width), jnp.bfloat16),
-            pltpu.VMEM((slot_names(dims)[1], seqs, width), jnp.bfloat16),
+            pltpu.VMEM((len(slot_names(dims)), seqs, width), jnp.bfloat16),
             pltpu.VMEM(expert_gate.shape[1:], expert_gate.dtype),
             pltpu.VMEM(expert_up.shape[1:], expert_up.dtype),
             pltpu.VMEM(expert_down.shape[1:], expert_down.dtype),

time: 72.3 us -> 67.4 us (0.932)
  Pallas kernels: 71.5 us -> 66.6 us
    pallas_call x1, Pallas kernels: 69.1 us -> 64.2 us  [shards(): pl.pallas_call(functools.partial(layer_kernel, dims, (heads, head_k, head...]
where the time goes in v2:
time: 67.4 us; the launch traced here: 67.3 us
  Pallas kernels  66.6 us (99%)
    pallas_call x1, Pallas kernels, shards(): pl.pallas_call(functools.partial(layer_kernel, dims, (heads, head_k, head...  64.2 us
    pallas_call x1, Pallas kernels, shards(): pl.pallas_call(give_kernel, out_shape=(jax.ShapeDtypeStruct((seqs, width)...  2.38 us

profile of v2, /device:TPU:0, one launch (start us, length us, event | category | flops | bytes accessed | tf_op | source)
XLA Modules:
  0.0 67.3 jit_solution(5427827876675105541)
XLA Ops:
  0.6 64.2 %layer.1 = (bf16[20,2048]{1,0:T(8,128)(2,1)S(1)}, f32[20,512,128]{2,1,0:T(8,128)S(1)}) custom-call(bf16[20,2048]{1,0:T(8,128)(2,1)} %tokens_hbm.1, s32[1,20]{1,0:T(1,128)} %bitcast.16, s32[6,20]{1,0:T(8,128)} %bitcast.13, f32[6,20]{1,0:T(8,128)} %bitcast.14, f32[1,2048]{1,0:T(1,128)} %bitcast.11, f32[1,1024]{1,0:T(1,128)} %bitcast.15, f32[1,2048]{1,0:T(1,128)} %bitcast.12, ...), custom_call_target="tpu_custom_call" | custom-call | tf_op jit(solution)/shard_map/layer/pallas_call | solution.py:700
  64.9 2.4 %give.1 = (bf16[20,2048]{1,0:T(8,128)(2,1)}, f32[20,512,128]{2,1,0:T(8,128)}) custom-call(bf16[20,2048]{1,0:T(8,128)(2,1)S(1)} %get-tuple-element.6.result, f32[20,512,128]{2,1,0:T(8,128)S(1)} %get-tuple-element.7.fresh), custom_call_target="tpu_custom_call" | custom-call | tf_op jit(solution)/shard_map/give/pallas_call | solution.py:748

commit v3 on v2

--- a/solution.py
+++ b/solution.py
@@ -116,7 +116,8 @@
 class Gather:
     def __init__(self, place, view, send, recv, split=True):
         self.place, self.view, self.send, self.recv = place, view, send, recv
-        self.direct = () if split else tuple(range(place.dims[0]))
+        singles, relays = stages(place.dims[0])
+        self.direct = tuple(singles[:1] + relays) if split else tuple(range(place.dims[0]))
         self.names = gather_names(place.dims)
         self.halves = (0, 1) if split else (0,)
         self.split = split
@@ -339,9 +340,14 @@
             c.wait_send()
 
 
+def stages(depth):
+    relays = [dz for dz in range(1, depth) if relay_bit(depth, dz)]
+    return [dz for dz in reversed(range(1, depth)) if dz not in relays], relays
+
+
 def plan(depth):
-    relays = [dz for dz in range(1, depth) if relay_bit(depth, dz)]
-    order = [0] + [dz for dz in reversed(range(1, depth)) if dz not in relays] + relays
+    singles, relays = stages(depth)
+    order = [0] + singles[:1] + relays + singles[1:]
     steps = []
 
     def say(kind, *planes):
@@ -352,26 +358,26 @@
     say("away", 0)
     say("first", 0)
     say("second", 0)
-    say("first", *[dz for dz in order[1:] if dz not in relays])
+    say("first", *singles)
     for i, dz in enumerate(order):
-        if i >= 1:
-            say("second", dz)
+        say("second", dz)
+        if i == 1:
             say("first", *relays)
-            say("second", *order[i + 1 : i + 2])
-        say("third", dz)
+            say("second", *singles)
+        if i == 2:
+            say("third", *singles)
+        if i >= 3:
+            say("add2", order[i - 2])
         if i >= 2:
             say("add1", order[i - 1])
-        if i >= 3:
-            say("add2", order[i - 2])
+        say("third", dz)
         say("fourth", dz)
         say("serve", dz)
-    say("add1", *order[1:])
-    say("add2", *order[-2:-1])
     say("add3", *order[1:-2])
-    say("add1", 0)
-    say("add2", *order[1:])
+    say("add2", *order[1:-1])
+    say("add1", *order[1:], 0)
     say("add3", *order[1:-1])
-    say("add2", 0)
+    say("add2", *order[1:], 0)
     say("add3", *order[1:], 0)
     return steps
 
@@ -515,8 +521,7 @@
         part = jnp.dot(normed, weight[...], preferred_element_type=jnp.float32)
         return part.astype(jnp.bfloat16).astype(jnp.float32)
 
-    singles = [dz for dz in reversed(range(1, depth)) if not relay_bit(depth, dz)]
-    relays = [dz for dz in range(1, depth) if relay_bit(depth, dz)]
+    singles, relays = stages(depth)
     weights[0].wait()
     columns(rotated(project(wq)), qcols)
     taken.start()
@@ -530,14 +535,15 @@
     taken.wait()
 
     def one(t, carry):
-        lane = lax.broadcasted_iota(jnp.int32, qcols.shape, 1)
-        query = jnp.sum(jnp.where(lane == t, qcols[...], 0.0), axis=1, keepdims=True)
-        key = jnp.sum(jnp.where(lane == t, kcols[...], 0.0), axis=1, keepdims=True)
+        where = jnp.full(qcols.shape, t, jnp.int32)
+        query = jnp.take_along_axis(qcols[...], where, axis=1, mode="promise_in_bounds")
+        key = jnp.take_along_axis(kcols[...], where, axis=1, mode="promise_in_bounds")
         value = values[t]
-        outer = key.reshape(heads, head_k, 1) * value.reshape(heads, 1, head_v)
+        shape = (heads, head_k, head_v)
+        outer = key.reshape(shape) * value.reshape(heads, 1, head_v)
         fresh = decay[...] * state[t] + outer.reshape(heads * head_k, head_v)
         state[t] = fresh
-        readout[t] = jnp.sum((query * fresh).reshape(heads, head_k, head_v), axis=1)
+        readout[t] = jnp.sum((query * fresh).reshape(shape), axis=1)
         return carry
 
     lax.fori_loop(0, seqs // 2, one, 0, unroll=2)

time: 67.4 us -> 66.4 us (0.985)
  Pallas kernels: 66.6 us -> 65.6 us
    pallas_call x1, Pallas kernels: 64.2 us -> 63.2 us  [shards(): pl.pallas_call(functools.partial(layer_kernel, dims, (heads, head_k, head...]
where the time goes in v3:
time: 66.4 us; the launch traced here: 66.3 us
  Pallas kernels  65.6 us (99%)
    pallas_call x1, Pallas kernels, shards(): pl.pallas_call(functools.partial(layer_kernel, dims, (heads, head_k, head...  63.2 us
    pallas_call x1, Pallas kernels, shards(): pl.pallas_call(give_kernel, out_shape=(jax.ShapeDtypeStruct((seqs, width)...  2.38 us

profile of v3, /device:TPU:0, one launch (start us, length us, event | category | flops | bytes accessed | tf_op | source)
XLA Modules:
  0.0 66.3 jit_solution(17590442704864281658)
XLA Ops:
  0.6 63.2 %layer.1 = (bf16[20,2048]{1,0:T(8,128)(2,1)S(1)}, f32[20,512,128]{2,1,0:T(8,128)S(1)}) custom-call(bf16[20,2048]{1,0:T(8,128)(2,1)} %tokens_hbm.1, s32[1,20]{1,0:T(1,128)} %bitcast.16, s32[6,20]{1,0:T(8,128)} %bitcast.13, f32[6,20]{1,0:T(8,128)} %bitcast.14, f32[1,2048]{1,0:T(1,128)} %bitcast.11, f32[1,1024]{1,0:T(1,128)} %bitcast.15, f32[1,2048]{1,0:T(1,128)} %bitcast.12, ...), custom_call_target="tpu_custom_call" | custom-call | tf_op jit(solution)/shard_map/layer/pallas_call | solution.py:706
  63.9 2.4 %give.1 = (bf16[20,2048]{1,0:T(8,128)(2,1)}, f32[20,512,128]{2,1,0:T(8,128)}) custom-call(bf16[20,2048]{1,0:T(8,128)(2,1)S(1)} %get-tuple-element.6.result, f32[20,512,128]{2,1,0:T(8,128)S(1)} %get-tuple-element.7.fresh), custom_call_target="tpu_custom_call" | custom-call | tf_op jit(solution)/shard_map/give/pallas_call | solution.py:754
